TPU v7x, 768 devices: a whole 4x8x12 slice. The times are simulated.
768 devices in a mesh: fs: 24 (over z, core), tp: 32 (over y, x).
Axes of the slice: x: 4, y: 8, z: 12, core: 2. Of those that a mesh axis runs over, the one named last changes fastest.
Arguments:
- trained_gate: float32 [32, 504, 2048], P(None, 'fs', 'tp'), may hold values from -0.125 to 0.125
- trained_up: float32 [32, 504, 2048], P(None, 'fs', 'tp'), may hold values from -0.125 to 0.125
- trained_down: float32 [32, 504, 2048], P(None, 'fs', 'tp'), may hold values from -0.25 to 0.25
- trained_shared_gate: float32 [504, 2048], P('fs', 'tp'), may hold values from -0.125 to 0.125
- trained_shared_up: float32 [504, 2048], P('fs', 'tp'), may hold values from -0.125 to 0.125
- trained_shared_down: float32 [504, 2048], P('fs', 'tp'), may hold values from -0.25 to 0.25
- ffn_gain: float32 [2048], P('tp'), may hold values from 0.1 to 1.9
- prompt_tokens: bfloat16 [6144, 2048], P('fs'), may hold values from -6 to 6
- expert_ids: int32 [6144, 8], P('fs'), may hold values from 0 to 31, all different within a row; in each aligned block of 256 rows (0 to 255, 256 to 511, ...) at most 160 rows name the same one
- route_scores: float32 [6144, 8], P('fs'), may hold values from 0.05 to 1
Outputs:
- served_gate: bfloat16 [32, 504, 2048], P('tp')
- served_up: bfloat16 [32, 504, 2048], P('tp')
- served_down: bfloat16 [32, 504, 2048], P('tp')
- served_shared_gate: bfloat16 [504, 2048], P(None, 'tp')
- served_shared_up: bfloat16 [504, 2048], P(None, 'tp')
- served_shared_down: bfloat16 [504, 2048], P(None, 'tp')
- mixture_out: bfloat16 [6144, 2048], P('fs', 'tp')
Inputs may be any that keep to these rules, and one draw needn't show every extreme that they name: `expert_ids`: each row names 8 different experts, and every expert is named by some row. Within the 256 rows of one index of fs no expert is named by more than 160 rows, and in every draw some expert is named by exactly 160 rows of some index of fs.
All inputs are finite; a program needn't handle non-finite values.
Results may differ from a plain program's by a relative error of at most 0.0082.
Values may be sent and summed in bfloat16 or wider, within the bound.
A program may use at most 64 MiB of HBM per device.

v0:
```python
import jax
import jax.numpy as jnp
from jax import lax
from jax.sharding import PartitionSpec as P

EPSILON = 1e-06
ROUTED_SCALE = 2.5


def side_by_side(arrays, axis, split_dim, concat_dim, along):
    ends, at = ([], 0)
    for a in arrays[:-1]:
        at += a.shape[along]
        ends.append(at)
    both = jnp.concatenate(arrays, axis=along)
    return tuple(
        jnp.split(
            lax.all_to_all(both, axis, split_axis=split_dim, concat_axis=concat_dim, tiled=True),
            ends,
            axis=along,
        )
    )


def packed_total(arrays, axis):
    ravelled, at, finished = (jnp.concatenate([a.reshape(-1) for a in arrays]), 0, [])
    subtotal = lax.psum(ravelled, axis)
    for a in arrays:
        finished.append(subtotal[at : at + a.size].reshape(a.shape))
        at += a.size
    return tuple(finished)


def split_up(x, dim, count):
    before, after = (x.shape[:dim], x.shape[dim + 1 :])
    return jnp.moveaxis(x.reshape(*before, count, -1, *after), dim, 0)


def summed_on_arrival(x, axis, dim):
    pieces = split_up(x, dim, lax.axis_size(axis))
    arrived = lax.all_to_all(pieces, axis, split_axis=0, concat_axis=0, tiled=True)
    return arrived.sum(axis=0)


def contract(left, right):
    return lax.dot_general(
        left, right, (((1,), (1,)), ((), ())), preferred_element_type=jnp.float32
    )


def on_device(
    trained_gate,
    trained_up,
    trained_down,
    trained_shared_gate,
    trained_shared_up,
    trained_shared_down,
    ffn_gain,
    prompt_tokens,
    expert_ids,
    route_scores,
):
    gate_cast = (trained_gate * ffn_gain[None, None, :]).astype(jnp.bfloat16)
    up_cast = (trained_up * ffn_gain[None, None, :]).astype(jnp.bfloat16)
    down_cast = trained_down.astype(jnp.bfloat16)
    shared_gate_cast = (trained_shared_gate * ffn_gain[None, :]).astype(jnp.bfloat16)[None]
    shared_up_cast = (trained_shared_up * ffn_gain[None, :]).astype(jnp.bfloat16)[None]
    shared_down_cast = trained_shared_down.astype(jnp.bfloat16)[None]
    expert_gate, expert_up, expert_down = side_by_side(
        (gate_cast, up_cast, down_cast), "tp", 0, 2, 1
    )
    token_count, model_width = prompt_tokens.shape
    tokens_float = prompt_tokens.astype(jnp.float32)
    normed = (
        tokens_float
        * lax.rsqrt(jnp.mean(tokens_float * tokens_float, axis=1, keepdims=True) + EPSILON)
    ).astype(jnp.bfloat16)
    column_width = ffn_gain.shape[0]
    expert_index = lax.axis_index("tp")
    normed_cols = lax.dynamic_slice_in_dim(normed, expert_index * column_width, column_width, 1)
    expert_count = lax.axis_size("tp")
    top_count = expert_ids.shape[1]
    capacity = min(token_count, 5 * token_count * top_count // (2 * expert_count))
    route_weight = ROUTED_SCALE * route_scores / jnp.sum(route_scores, axis=1, keepdims=True)
    chosen = expert_ids == expert_index
    token_weight = jnp.sum(jnp.where(chosen, route_weight, 0.0), axis=1)
    present = jnp.any(chosen, axis=1)
    position = jnp.cumsum(present.astype(jnp.int32)) - 1
    slot_match = (position[None, :] == jnp.arange(capacity, dtype=jnp.int32)[:, None]) & present[
        None, :
    ]
    slot_token = jnp.sum(
        jnp.where(slot_match, jnp.arange(token_count, dtype=jnp.int32)[None, :], 0), axis=1
    )
    slot_rows = jnp.take(normed, slot_token, axis=0)
    gathered = (
        lax.all_gather(expert_gate, "fs", axis=1, tiled=True),
        lax.all_gather(expert_up, "fs", axis=1, tiled=True),
        lax.all_gather(expert_down, "fs", axis=1, tiled=True),
        lax.all_gather(shared_gate_cast, "fs", axis=1, tiled=True),
        lax.all_gather(shared_up_cast, "fs", axis=1, tiled=True),
        lax.all_gather(shared_down_cast, "fs", axis=1, tiled=True),
    )
    gate_full, up_full, down_full, sgate_full, sup_full, sdown_full = gathered
    gate_pre = contract(slot_rows, gate_full[0])
    up_pre = contract(slot_rows, up_full[0])
    sgate_part = contract(normed_cols, sgate_full[0])
    sup_part = contract(normed_cols, sup_full[0])
    expert_act = (jax.nn.silu(gate_pre) * up_pre).astype(jnp.bfloat16)
    shared_gate_pre, shared_up_pre = packed_total((sgate_part, sup_part), "tp")
    shared_act = (jax.nn.silu(shared_gate_pre) * shared_up_pre).astype(jnp.bfloat16)
    expert_out = jnp.dot(expert_act, down_full[0], preferred_element_type=jnp.float32)
    shared_out = jnp.dot(shared_act, sdown_full[0], preferred_element_type=jnp.float32)
    picked = jnp.take(expert_out, jnp.maximum(position, 0), axis=0)
    routed_part = jnp.where(present[:, None], picked * token_weight[:, None], 0.0)
    routed_cols = summed_on_arrival(routed_part, "tp", 1)
    mixture = (routed_cols + shared_out).astype(jnp.bfloat16)
    return (gate_full, up_full, down_full, sgate_full[0], sup_full[0], sdown_full[0], mixture)


def solution(mesh):
    placed = (
        P(None, "fs", "tp"),
        P(None, "fs", "tp"),
        P(None, "fs", "tp"),
        P("fs", "tp"),
        P("fs", "tp"),
        P("fs", "tp"),
        P("tp"),
        P("fs", None),
        P("fs", None),
        P("fs", None),
    )
    return jax.shard_map(
        on_device,
        mesh=mesh,
        in_specs=placed,
        out_specs=(
            P("tp", None, None),
            P("tp", None, None),
            P("tp", None, None),
            P(None, "tp"),
            P(None, "tp"),
            P(None, "tp"),
            P("fs", "tp"),
        ),
        check_vma=False,
    )
```

profile of v0, /device:TPU:1, one launch (start us, length us, event | category | flops | bytes accessed | tf_op | source)
XLA Modules:
  0.0 307.0 jit_solution(18084856175359266622)
XLA Ops:
  8.0 1.0 convert_element_type.42
  9.1 1.2 multiply_convert_fusion.2
  10.9 20.7 %all_to_all.23 = bf16[32,2,2016]{2,1,0:T(2,128)(2,1)S(1)} all-to-all(bf16[32,2,2016]{2,1,0:T(2,128)(2,1)S(1)} %reshape.183), channel_id=1, replica_groups=mesh['fs'=24,'tp'=32] {'tp'}, dimensions={0} | all-to-all | bytes 516096 | tf_op jit(solution)/shard_map/all_to_all | solution.py:18
  32.8 0.8 copy.72
  33.7 0.8 copy.74
  34.7 36.8 %all-gather.4 = bf16[24,21,64]{2,1,0:T(8,128)(2,1)S(1)} all-gather(bf16[1,21,64]{2,1,0:T(8,128)(2,1)S(1)} %get-tuple-element.51), channel_id=3, replica_groups=mesh['fs'=24,'tp'=32] {'fs'}, dimensions={0}, use_global_device_ids=true | all-gather | bytes 67200 | tf_op jit(solution)/shard_map/all_gather | solution.py:101
  72.1 0.8 copy.73
  73.2 21.5 %all-gather.3 = bf16[24,21,64]{2,1,0:T(8,128)(2,1)S(1)} all-gather(bf16[1,21,64]{2,1,0:T(8,128)(2,1)S(1)} %get-tuple-element.52), channel_id=2, replica_groups=mesh['fs'=24,'tp'=32] {'fs'}, dimensions={0}, use_global_device_ids=true | all-gather | bytes 67200 | tf_op jit(solution)/shard_map/all_gather | solution.py:100
  96.1 1.0 pad_maximum_fusion
  98.2 1.0 gather_fusion
  99.2 0.6 all-gather.10.cloned.1.call-done
  99.8 3.4 %copy.78 = bf16[1,504,2048]{2,1,0:T(8,128)(2,1)S(1)} copy(bf16[1,504,2048]{2,0,1:T(2,128)(2,1)} %all-gather.10.cloned.1.call-done) | data formatting | bytes 4128768
  103.3 1.3 copy-done.1
  104.6 1.6 fusion.6
  106.2 55.4 %all-gather.14.cloned.1.call-done = bf16[1,504,2048]{2,0,1:T(2,128)(2,1)} async-done(((bf16[1,21,2048]{2,0,1:T(2,128)(2,1)}), bf16[1,504,2048]{2,0,1:T(2,128)(2,1)}) %all-gather.14.cloned.1.call-update) | async-done | bytes 2064400 | tf_op jit(solution)/shard_map/all_gather | solution.py:99
  161.6 3.4 %copy.80 = bf16[1,504,2048]{2,1,0:T(8,128)(2,1)S(1)} copy(bf16[1,504,2048]{2,0,1:T(2,128)(2,1)} %all-gather.14.cloned.1.call-done) | data formatting | bytes 4128768
  165.0 58.8 %all-gather.12.cloned.1.call-done = bf16[1,504,2048]{2,0,1:T(2,128)(2,1)} async-done(((bf16[1,21,2048]{2,0,1:T(2,128)(2,1)}), bf16[1,504,2048]{2,0,1:T(2,128)(2,1)}) %all-gather.12.cloned.1.call-update) | async-done | bytes 2064400 | tf_op jit(solution)/shard_map/all_gather | solution.py:98
  223.8 4.7 %copy.79 = bf16[1,504,2048]{2,1,0:T(8,128)(2,1)} copy(bf16[1,504,2048]{2,0,1:T(2,128)(2,1)} %all-gather.12.cloned.1.call-done) | data formatting | bytes 4128768
  228.5 3.1 %fusion.2 = f32[160,2048]{1,0:T(8,128)S(1)} fusion(bf16[1,504,2048]{2,1,0:T(8,128)(2,1)S(1)} %copy.80, bf16[1,504,2048]{2,1,0:T(8,128)(2,1)} %copy.79, f32[160,504]{1,0:T(8,128)} %fusion.6, bf16[160,2048]{1,0:T(8,128)(2,1)} %copy-done.5, pred[160]{0:T(512)(128)(4,1)S(1)} %compare_and_fusion), kind=kOutput, calls=%fused_computation.7 | convolution fusion | flops 661414400 | bytes 6417568 | tf_op jit(solution)/shard_map/dot_general | solution.py:112
  231.7 1.5 gather_fusion.1
  233.2 1.8 copy.75
  235.0 3.3 %select_bitcast_fusion = f32[32,256,64]{1,2,0:T(8,128)} fusion(f32[256,32,64]{0,2,1:T(8,128)} %bitcast.41, f32[256]{0:T(256)S(1)} %get-tuple-element.44, pred[256]{0:T(512)(128)(4,1)S(1)} %get-tuple-element.42, pred[256]{0:T(512)(128)(4,1)S(1)} %reduce_or.9), kind=kLoop, calls=%fused_computation.6 | loop fusion | flops 1572864 | bytes 4195840 | tf_op jit(solution)/shard_map/transpose | solution.py:36
  238.3 9.4 %all-to-all-start.1 = ((f32[32,256,64]{1,2,0:T(8,128)}), f32[32,256,64]{1,2,0:T(8,128)S(1)}, u32[]{:S(2)}, u32[]{:S(2)}) async-start(f32[32,256,64]{1,2,0:T(8,128)} %select_bitcast_fusion), calls=%async_computation.1 | async-start | bytes 4194304 | tf_op jit(solution)/shard_map/all_to_all | solution.py:41
  247.7 0.8 copy.82
  248.4 0.8 copy.81
  249.2 22.4 %all-gather.5 = bf16[24,21,64]{2,1,0:T(8,128)(2,1)S(1)} all-gather(bf16[1,21,64]{2,1,0:T(8,128)(2,1)S(1)} %convert_bitcast_fusion), channel_id=4, replica_groups=mesh['fs'=24,'tp'=32] {'fs'}, dimensions={0}, use_global_device_ids=true | all-gather | bytes 67200 | tf_op jit(solution)/shard_map/all_gather | solution.py:102
  271.7 0.8 copy.83
  272.4 1.3 fusion.39
  273.7 1.3 slice.36
  275.0 1.3 slice.38
  276.3 21.5 %all-to-all-done.1 = f32[32,256,64]{1,2,0:T(8,128)S(1)} async-done(((f32[32,256,64]{1,2,0:T(8,128)}), f32[32,256,64]{1,2,0:T(8,128)S(1)}, u32[]{:S(2)}, u32[]{:S(2)}) %all-to-all-start.1) | async-done | bytes 2097184 | tf_op jit(solution)/shard_map/all_to_all | solution.py:41
  297.9 2.0 fusion.16
  (69 shorter events, 5.5 us)
Async XLA Ops:
  8.0 91.8 %all-gather.10.cloned.1.call-start = ((), (), s32[]{:S(2)}) async-start(), calls=%async_computation.2 | async-start | bytes 4300800 | tf_op jit(solution)/shard_map/all_gather | solution.py:97
  31.6 3.0 copy-start.9
  31.6 3.0 copy-start.10
  31.6 3.0 copy-start.12
  31.6 39.9 %copy-start = (bf16[256,2048]{1,0:T(8,128)(2,1)S(1)}, bf16[256,2048]{1,0:T(8,128)(2,1)}, u32[]{:S(2)}) copy-start(bf16[256,2048]{1,0:T(8,128)(2,1)} %param.17) | copy-start | bytes 3145732
  33.7 127.9 %all-gather.14.cloned.1.call-start = ((), (), s32[]{:S(2)}) async-start(), calls=%async_computation.4 | async-start | bytes 4300800 | tf_op jit(solution)/shard_map/all_gather | solution.py:99
  34.6 189.2 %all-gather.12.cloned.1.call-start = ((), (), s32[]{:S(2)}) async-start(), calls=%async_computation.3 | async-start | bytes 4300800 | tf_op jit(solution)/shard_map/all_gather | solution.py:98
  72.9 199.5 %all-reduce.2.cloned.1.call-start = ((), (), s32[]{:S(2)}) async-start(), calls=%async_computation.5 | async-start | bytes 2064384 | tf_op jit(solution)/shard_map/psum | solution.py:27
  94.8 0.7 copy-start.3
  95.7 1.5 copy-start.7
  95.7 1.5 copy-start.11
  99.2 4.1 %copy-start.5 = (bf16[160,2048]{1,0:T(8,128)(2,1)}, bf16[160,2048]{1,0:T(8,128)(2,1)S(1)}, u32[]{:S(2)}) copy-start(bf16[160,2048]{1,0:T(8,128)(2,1)S(1)} %gather_fusion) | copy-start | bytes 1966084
  103.3 1.3 copy-start.1
  165.0 63.5 %copy-start.2 = (bf16[1,504,2048]{2,1,0:T(8,128)(2,1)}, bf16[1,504,2048]{2,1,0:T(8,128)(2,1)S(1)}, u32[]{:S(2)}) copy-start(bf16[1,504,2048]{2,1,0:T(8,128)(2,1)S(1)} %copy.80) | copy-start | bytes 6193156
  238.3 10.2 %copy-start.4 = (bf16[504,64]{1,0:T(8,128)(2,1)S(1)}, bf16[504,64]{1,0:T(8,128)(2,1)}, u32[]{:S(2)}) copy-start(bf16[504,64]{1,0:T(8,128)(2,1)} %copy-done.3) | copy-start | bytes 193540
  238.3 10.9 %copy-start.8 = (f32[21,64]{1,0:T(8,128)S(1)}, f32[21,64]{1,0:T(8,128)}, u32[]{:S(2)}) copy-start(f32[21,64]{1,0:T(8,128)} %param.15) | copy-start | bytes 16132
  238.3 59.5 %all-to-all-start.1 = ((f32[32,256,64]{1,2,0:T(8,128)}), f32[32,256,64]{1,2,0:T(8,128)S(1)}, u32[]{:S(2)}, u32[]{:S(2)}) async-start(f32[32,256,64]{1,2,0:T(8,128)} %select_bitcast_fusion), calls=%async_computation.1 | async-start | bytes 4194304 | tf_op jit(solution)/shard_map/all_to_all | solution.py:41
  275.0 22.9 %copy-start.6 = (f32[256,504]{1,0:T(8,128)S(1)}, f32[256,504]{1,0:T(8,128)}, u32[]{:S(2)}) copy-start(f32[256,504]{1,0:T(8,128)} %slice.36) | copy-start | bytes 1548292
Sparse Core Ops, SparseCore 0:
  33.8 66.0 all-gather.9
  102.3 59.2 all-gather.13
  164.6 59.1 all-gather.11
Sparse Core Ops, SparseCore 1:
  97.3 157.4 all-reduce.1
where the time goes:
time: 308 us; the launch traced here: 307 us
  waiting for transfers between devices  136 us (44%)
  blocking collectives  101 us (33%)
  local copies, waits for them, and re-layouts  29 us (9%)
  between operations  15.5 us (5%)
  starting transfers between devices  9.54 us (3%)
  other arithmetic  7.98 us (3%)
  matrix products  7.27 us (2%)
    all_gather x1, waiting for transfers between devices, on_device(): lax.all_gather(expert_up, 'fs', axis=1, tiled=True)  58.8 us
    all_gather x1, waiting for transfers between devices, on_device(): lax.all_gather(expert_down, 'fs', axis=1, tiled=True)  55.4 us
    all_gather x1, blocking collectives, on_device(): lax.all_gather(shared_up_cast, 'fs', axis=1, tiled=True)  36.8 us
    all_gather x1, blocking collectives, on_device(): lax.all_gather(shared_down_cast, 'fs', axis=1, tiled=True)  22.4 us
    all_gather x1, blocking collectives, on_device(): lax.all_gather(shared_gate_cast, 'fs', axis=1, tiled=True)  21.5 us
    all_to_all x1, waiting for transfers between devices, summed_on_arrival(): lax.all_to_all(pieces, axis, split_axis=0, concat_axis=0, tiled=True)  21.5 us
    all_to_all x1, blocking collectives, side_by_side(): lax.all_to_all(both, axis, split_axis=split_dim, concat_axis=concat_dim,...  20.7 us
    unnamed x37, local copies, waits for them, and re-layouts  16.3 us
  transfers between devices with their start and end apart: 5, of which 4 were waited for; matrix products, arithmetic and copies ran while one was open for 12% of the time, Pallas kernels for 0%

commit v1 on v0

v1 whole, which is shorter than its diff:
```python
import functools

import jax
import jax.numpy as jnp
from jax import lax
from jax.experimental import pallas as pl
from jax.experimental.pallas import tpu as pltpu
from jax.sharding import PartitionSpec as P

EPSILON = 1e-06
ROUTED_SCALE = 2.5
MESH = pl.DeviceIdType.MESH
NX = 4
CHUNKS = 4
ROW = 64
F32, BF16 = jnp.float32, jnp.bfloat16


def nt(a, b):
    return lax.dot_general(a, b, (((1,), (1,)), ((), ())), preferred_element_type=F32)


def tn(a, b):
    return lax.dot_general(a, b, (((0,), (0,)), ((), ())), preferred_element_type=F32)


def nn(a, b):
    return jnp.dot(a, b, preferred_element_type=F32)


def iota(shape, dim):
    return lax.broadcasted_iota(jnp.int32, shape, dim)


def silu(v):
    return v / (1.0 + jnp.exp(-v))


def halves(a, b):
    low = iota(a.shape, len(a.shape) - 1) < 64
    ax = len(a.shape) - 1
    return (
        jnp.where(low, a, pltpu.roll(b, 64, ax)),
        jnp.where(low, pltpu.roll(a, 64, ax), b),
    )


def kernel(
    n_tp, nz, units, cap,
    tg, tu, td, sg, su, sd, gain, tok, ids, scores,
    o_gate, o_up, o_down, o_sgate, o_sup, o_sdown, o_mix,
    send_a, recv_a, blocks, small, normed, rows, total, spread, slot_weight,
    pre_send, pre_recv, acts, sdown, send_x, recv_x, send_y, recv_y, staged,
    sem_a, sem_ring_s, sem_ring_r, sem_pair_s, sem_pair_r,
    sem_small_s, sem_small_r, sem_spair, sem_j, sem_act, sem_x_s, sem_x_r, sem_y_s, sem_y_r,
    sem_out,
):
    n_y = n_tp // NX
    far = nz // 2
    groups = nz // 4
    group_rows = 8 * units
    hidden = nz * 2 * units
    per_j = pre_send.shape[1]
    width = total.shape[1]
    tokens = tok.shape[0]
    me = lax.axis_index("tp")
    fs = lax.axis_index("fs")
    z, core = fs // 2, lax.rem(fs, 2)
    y, x = me // NX, lax.rem(me, NX)
    ahead = lax.rem(z + 1, nz) * 2 + core
    behind = lax.rem(z + nz - 1, nz) * 2 + core
    twin = z * 2 + 1 - core

    barrier = pltpu.get_barrier_semaphore()

    def greet(i, _):
        peer = lax.rem(me + i, n_tp)
        pl.semaphore_signal(barrier, inc=1, device_id={"tp": peer}, device_id_type=MESH)
        return 0

    for other in (ahead, behind, twin):
        pl.semaphore_signal(barrier, inc=1, device_id={"fs": other}, device_id_type=MESH)
    lax.fori_loop(1, n_tp, greet, 0)

    def pack(g, u, d):
        stack = jnp.concatenate([g, u, d, jnp.zeros((ROW - 3 * units, 64), F32)], axis=0)
        return jnp.concatenate([stack[: ROW // 2], stack[ROW // 2 :]], axis=1).astype(BF16)

    scale = gain[...]

    def prepare(e, _):
        send_a[e] = pack(tg[e] * scale, tu[e] * scale, td[e])
        return 0

    small[z, core] = pack(sg[...] * scale, su[...] * scale, sd[...])
    lax.fori_loop(0, n_tp, prepare, 0)
    recv_a[me] = send_a[me]
    pl.semaphore_wait(barrier, n_tp + 2)

    def plane(src, dst, sems, peer):
        return pltpu.make_async_remote_copy(
            src_ref=src, dst_ref=dst, send_sem=sems.at[0], recv_sem=sems.at[1],
            device_id={"tp": peer}, device_id_type=MESH,
        )

    def plane_done(ref, sems):
        piece = ref.at[pl.ds(0, n_tp - 1)]
        done = plane(piece, piece, sems, lax.rem(me + 1, n_tp))
        done.wait_send()
        done.wait_recv()

    def small_hop(d, s, at):
        return pltpu.make_async_remote_copy(
            src_ref=small.at[at, core], dst_ref=small.at[at, core],
            send_sem=sem_small_s.at[d, s], recv_sem=sem_small_r.at[d, s],
            device_id={"fs": ahead if d == 0 else behind}, device_id_type=MESH,
        )

    def small_pair(at):
        return pltpu.make_async_remote_copy(
            src_ref=small.at[at, core], dst_ref=small.at[at, core],
            send_sem=sem_spair.at[0], recv_sem=sem_spair.at[1],
            device_id={"fs": twin}, device_id_type=MESH,
        )

    def origin(d, s):
        return lax.rem(z + nz - s, nz) if d == 0 else lax.rem(z + s, nz)

    small_hop(0, 1, z).start()
    small_hop(1, 1, z).start()
    small_pair(z).start()

    def send_weights(i, _):
        peer = lax.rem(me + i, n_tp)
        plane(send_a.at[peer], recv_a.at[me], sem_a, peer).start()
        return 0

    lax.fori_loop(1, n_tp, send_weights, 0)

    def small_step(s):
        for d in (0, 1):

            def arrived(d=d):
                at = origin(d, s)
                small_hop(d, s, at).wait_recv()
                small_pair(at).start()

                @pl.when((s + 1 < far) | ((s + 1 == far) & (d == 0)))
                def _():
                    small_hop(d, s + 1, at).start()

            if d == 0:
                arrived()
            else:
                pl.when(s < far)(arrived)

    tf = tok[...].astype(F32)
    normed[...] = (
        tf * lax.rsqrt(jnp.mean(tf * tf, axis=1, keepdims=True) + EPSILON)
    ).astype(BF16)
    ids_v, sc = ids[...], scores[...]
    ratio = ROUTED_SCALE * sc / jnp.sum(sc, axis=1, keepdims=True)
    lane = iota((tokens, 128), 1)
    present = jnp.zeros((tokens, 128), F32)
    weight = jnp.zeros((tokens, 128), F32)
    for k in range(ids.shape[1]):
        hit = ids_v[:, k : k + 1] == lane
        present = jnp.where(hit, 1.0, present)
        weight = jnp.where(hit, weight + ratio[:, k : k + 1], weight)
    before = jnp.where(iota((tokens, tokens), 1) < iota((tokens, tokens), 0), 1.0, 0.0)
    position = nn(before.astype(BF16), present.astype(BF16))
    slot = jnp.where(present > 0.0, position, -1.0)
    mine = iota((128, tokens), 0) == me
    slot_row = jnp.sum(jnp.where(mine, slot.T, 0.0), axis=0, keepdims=True)
    weight_row = jnp.sum(jnp.where(mine, weight.T, 0.0), axis=0, keepdims=True)
    taken = slot_row == iota((cap, tokens), 0).astype(F32)
    slot_weight[...] = jnp.broadcast_to(
        jnp.sum(jnp.where(taken, weight_row, 0.0), axis=1, keepdims=True), slot_weight.shape
    )
    rows[...] = nn(jnp.where(taken, 1.0, 0.0).astype(BF16), normed[...]).astype(BF16)
    for i in range(NX):
        col = jnp.sum(jnp.where(lane == y * NX + i, slot, 0.0), axis=1, keepdims=True)
        spread[i] = jnp.where(col == iota((tokens, cap), 1).astype(F32), 1.0, 0.0).astype(BF16)
    total[...] = jnp.zeros_like(total)

    small_step(1)
    plane_done(recv_a, sem_a)

    for m in range(n_tp // 2):
        top, low = halves(recv_a[2 * m].astype(F32), recv_a[2 * m + 1].astype(F32))
        whole = jnp.concatenate([top, low], axis=0)
        blocks[z, core, :, pl.ds(128 * m, 128)] = whole.astype(BF16)

    size = ROW // CHUNKS

    def hop(d, s, q, at):
        piece = blocks.at[at, core, pl.ds(q * size, size)]
        return pltpu.make_async_remote_copy(
            src_ref=piece, dst_ref=piece,
            send_sem=sem_ring_s.at[d, s, q], recv_sem=sem_ring_r.at[d, s, q],
            device_id={"fs": ahead if d == 0 else behind}, device_id_type=MESH,
        )

    def pair(at):
        rel = lax.rem(at + nz - z, nz)
        return pltpu.make_async_remote_copy(
            src_ref=blocks.at[at, core], dst_ref=blocks.at[at, core],
            send_sem=sem_pair_s.at[rel], recv_sem=sem_pair_r.at[rel],
            device_id={"fs": twin}, device_id_type=MESH,
        )

    for q in range(CHUNKS):
        for d in (0, 1):
            hop(d, 1, q, z).start()
    pair(z).start()

    def last_leg(d, q):
        return (q < CHUNKS // 2) == (d == 0)

    def expert(at):
        pair(at).wait_recv()
        w = blocks[at].reshape(2 * ROW, width)
        pre = nt(rows[...], w)
        act = silu(pltpu.roll(pre, 2 * units, 1)) * pltpu.roll(pre, units, 1)
        unit = iota(act.shape, 1) & (ROW - 1)
        act = jnp.where((unit >= 2 * units) & (unit < 3 * units), act, 0.0).astype(BF16)
        total[...] += nn(act, w)

    def picks():
        shape = (group_rows, 8 * ROW)
        i, c = iota(shape, 0), iota(shape, 1)
        f, r = c // ROW, c & (ROW - 1)
        return [
            jnp.where((r >= units * m) & (r < units * (m + 1)) & (i == units * f + r - units * m), 1.0, 0.0).astype(BF16)
            for m in range(3)
        ]

    def shared_rows():
        def spent(i, _):
            small_pair(z).wait_recv()
            return 0

        got = [[], [], []]
        for g in range(groups):
            v = small[pl.ds(4 * g, 4)].reshape(8, ROW // 2, 128).astype(F32)
            v = jnp.concatenate([v, pltpu.roll(v, 64, 2)], axis=1).reshape(8 * ROW, 128)
            v = v.astype(BF16)
            for m, p in enumerate(picks()):
                got[m].append(nn(p, v))
        gate, up, down = [jnp.concatenate(one, axis=0) for one in got]
        for o, v in ((o_sgate, gate), (o_sup, up), (o_sdown, down)):
            o[...] = v[:, :64].astype(BF16)
        pad = jnp.zeros((n_tp * per_j - hidden, 128), F32)
        both = jnp.concatenate([halves(gate, up)[0], pad], axis=0)
        pre_send[...] = both.astype(BF16).reshape(n_tp, per_j, 128)
        low = iota(down.shape, 1) < 64
        down = jnp.concatenate([jnp.where(low, down, 0.0), pad], axis=0)
        sdown[...] = down.astype(BF16)
        pre_recv[me] = pre_send[me]

        def send(i, _):
            peer = lax.rem(me + i, n_tp)
            plane(pre_send.at[peer], pre_recv.at[me], sem_j, peer).start()
            return 0

        lax.fori_loop(1, n_tp, send, 0)

    def ring_step(s, _):
        for q in range(CHUNKS):
            for d in (0, 1):

                def arrived(d=d, q=q):
                    at = origin(d, s)
                    hop(d, s, q, at).wait_recv()
                    go = s + 1 <= far if last_leg(d, q) else s + 1 < far

                    @pl.when(go)
                    def _():
                        hop(d, s + 1, q, at).start()

                if last_leg(d, q):
                    arrived()
                else:
                    pl.when(s < far)(arrived)
        pair(origin(0, s)).start()

        @pl.when(s < far)
        def _():
            pair(origin(1, s)).start()

        @pl.when(s < far)
        def _():
            small_step(s + 1)

        def one(i, _):
            expert(lax.rem(z + nz + (s - 1) * (1 - 2 * i), nz))
            return 0

        lax.fori_loop(0, jnp.where(s == 1, 1, 2), one, 0)

        @pl.when(s == far)
        def _():
            everything = small.at[:, 0]
            done = pltpu.make_async_remote_copy(
                src_ref=everything, dst_ref=everything,
                send_sem=sem_spair.at[0], recv_sem=sem_spair.at[1],
                device_id={"fs": twin}, device_id_type=MESH,
            )
            done.wait_send()
            done.wait_recv()
            shared_rows()

        return 0

    lax.fori_loop(1, far + 1, ring_step, 0)
    expert(lax.rem(z + far, nz))

    w = slot_weight[...]
    for p in range(n_y // 2):
        for h in range(NX // 2):
            a = total[:, pl.ds(128 * (2 * p * (NX // 2) + h), 128)] * w
            b = total[:, pl.ds(128 * ((2 * p + 1) * (NX // 2) + h), 128)] * w
            left, right = halves(a, b)
            send_x[2 * h, :, pl.ds(128 * p, 128)] = left.astype(BF16)
            send_x[2 * h + 1, :, pl.ds(128 * p, 128)] = right.astype(BF16)

    def row_copy(i):
        to = lax.rem(x + i, NX)
        return pltpu.make_async_remote_copy(
            src_ref=send_x.at[to], dst_ref=recv_x.at[x],
            send_sem=sem_x_s.at[i], recv_sem=sem_x_r.at[i],
            device_id={"tp": y * NX + to}, device_id_type=MESH,
        )

    for i in range(1, NX):
        row_copy(i).start()
    recv_x[x] = send_x[x]

    plane_done(pre_recv, sem_j)
    gates, ups = [], []
    for m in range(n_tp // 2):
        g, u = halves(pre_recv[2 * m].astype(F32), pre_recv[2 * m + 1].astype(F32))
        gates.append(g.astype(BF16))
        ups.append(u.astype(BF16))
    gate = nt(jnp.concatenate(gates, axis=1), normed[...])
    up = nt(jnp.concatenate(ups, axis=1), normed[...])
    acts[me] = (silu(gate) * up).astype(BF16)

    def send_act(i, _):
        peer = lax.rem(me + i, n_tp)
        plane(acts.at[me], acts.at[me], sem_act, peer).start()
        return 0

    lax.fori_loop(1, n_tp, send_act, 0)

    part = min(512, width)
    steps = width // part
    outs = (o_gate, o_up, o_down)

    def leave(m, g):
        return pltpu.make_async_copy(staged.at[m, g], outs[m].at[g], sem_out.at[m, g])

    for g in range(groups):
        for m, p in enumerate(picks()):

            def served(n, _, m=m, g=g, p=p):
                cols = pl.ds(pl.multiple_of(n * part, part), part)
                v = blocks[pl.ds(4 * g, 4), :, :, cols].reshape(8 * ROW, part)
                staged[m, g, :, cols] = nn(p, v).astype(BF16)
                return 0

            lax.fori_loop(0, steps, served, 0)
            leave(m, g).start()

    for i in range(1, NX):
        row_copy(i).wait_send()
        row_copy(i).wait_recv()

    half = tokens // 2
    for p in range(n_y // 2):
        acc = jnp.zeros((tokens, 128), F32)
        for i in range(NX):
            acc += nn(spread[i], recv_x[i, :, pl.ds(128 * p, 128)])
        left, right = halves(acc[:half], acc[half:])
        send_y[2 * p] = left.astype(BF16)
        send_y[2 * p + 1] = right.astype(BF16)

    def col_copy(i):
        to = lax.rem(y + i, n_y)
        return pltpu.make_async_remote_copy(
            src_ref=send_y.at[to], dst_ref=recv_y.at[y],
            send_sem=sem_y_s.at[i], recv_sem=sem_y_r.at[i],
            device_id={"tp": to * NX + x}, device_id_type=MESH,
        )

    for i in range(1, n_y):
        col_copy(i).start()
    recv_y[y] = send_y[y]

    def act_done():
        piece = acts.at[pl.ds(0, n_tp - 1)]
        done = plane(piece, piece, sem_act, lax.rem(me + 1, n_tp))
        done.wait_send()
        done.wait_recv()

    act_done()
    shared = tn(acts[...].reshape(n_tp * per_j, tokens), sdown[...])
    mixed = halves(shared[:half], shared[half:])[0]
    for i in range(1, n_y):
        col_copy(i).wait_send()
        col_copy(i).wait_recv()
    for i in range(n_y):
        mixed += recv_y[i].astype(F32)
    upper = pltpu.roll(mixed, 64, 1)
    o_mix[...] = jnp.concatenate([mixed[:, :64], upper[:, :64]], axis=0).astype(BF16)

    for d in (0, 1):
        for q in range(CHUNKS):

            def sent(s, _, d=d, q=q):
                hop(d, s, q, z).wait_send()
                return 0

            lax.fori_loop(1, far + (1 if last_leg(d, q) else 0), sent, 0)

        def small_sent(s, _, d=d):
            small_hop(d, s, z).wait_send()
            return 0

        lax.fori_loop(1, far + (1 if d == 0 else 0), small_sent, 0)

    def pair_sent(i, _):
        pair(i).wait_send()
        return 0

    lax.fori_loop(0, nz, pair_sent, 0)
    for g in range(groups):
        for m in range(3):
            leave(m, g).wait()


def on_device(*args):
    tg, ids = args[0], args[8]
    n_tp, units = tg.shape[0], tg.shape[1]
    nz = lax.axis_size("fs") // 2
    tokens, width = args[7].shape
    top = ids.shape[1]
    cap = min(tokens, 5 * tokens * top // (2 * n_tp))
    hidden = nz * 2 * units
    per_j = -(-hidden // (16 * n_tp)) * 16
    n_y = n_tp // NX
    far = nz // 2
    groups = nz // 4
    args = list(args)
    args[6] = args[6].reshape(1, -1)
    vm = pl.BlockSpec(memory_space=pltpu.VMEM)
    hbm = pl.BlockSpec(memory_space=pl.ANY)
    dma = pltpu.SemaphoreType.DMA
    big = jax.ShapeDtypeStruct((groups, 8 * units, width), BF16)
    thin = jax.ShapeDtypeStruct((hidden, 64), BF16)
    outs = pl.pallas_call(
        functools.partial(kernel, n_tp, nz, units, cap),
        name="hand_over",
        out_shape=[big, big, big, thin, thin, thin, jax.ShapeDtypeStruct((tokens, 64), BF16)],
        in_specs=[vm] * 10,
        out_specs=[hbm] * 3 + [vm] * 4,
        scratch_shapes=[
            pltpu.VMEM((n_tp, ROW // 2, 128), BF16),
            pltpu.VMEM((n_tp, ROW // 2, 128), BF16),
            pltpu.VMEM((nz, 2, ROW, width), BF16),
            pltpu.VMEM((nz, 2, ROW // 2, 128), BF16),
            pltpu.VMEM((tokens, width), BF16),
            pltpu.VMEM((cap, width), BF16),
            pltpu.VMEM((cap, width), F32),
            pltpu.VMEM((NX, tokens, cap), BF16),
            pltpu.VMEM((cap, 128), F32),
            pltpu.VMEM((n_tp, per_j, 128), BF16),
            pltpu.VMEM((n_tp, per_j, 128), BF16),
            pltpu.VMEM((n_tp, per_j, tokens), BF16),
            pltpu.VMEM((n_tp * per_j, 128), BF16),
            pltpu.VMEM((NX, cap, 64 * n_y), BF16),
            pltpu.VMEM((NX, cap, 64 * n_y), BF16),
            pltpu.VMEM((n_y, tokens // 2, 128), BF16),
            pltpu.VMEM((n_y, tokens // 2, 128), BF16),
            pltpu.VMEM((3, groups, 8 * units, width), BF16),
            dma((2,)),
            dma((2, far + 1, CHUNKS)),
            dma((2, far + 1, CHUNKS)),
            dma((nz,)),
            dma((nz,)),
            dma((2, far + 1)),
            dma((2, far + 1)),
            dma((2,)),
            dma((2,)),
            dma((2,)),
            dma((NX,)),
            dma((NX,)),
            dma((n_y,)),
            dma((n_y,)),
            dma((3, groups)),
        ],
        compiler_params=pltpu.CompilerParams(
            collective_id=0, has_side_effects=True, vmem_limit_bytes=56 * 1024 * 1024
        ),
    )(*args)
    gate, up, down, sgate, sup, sdown, mixture = outs
    full = [v.reshape(1, hidden, width) for v in (gate, up, down)]
    return (*full, sgate, sup, sdown, mixture)


def solution(mesh):
    placed = (
        P(None, "fs", "tp"),
        P(None, "fs", "tp"),
        P(None, "fs", "tp"),
        P("fs", "tp"),
        P("fs", "tp"),
        P("fs", "tp"),
        P("tp"),
        P("fs", None),
        P("fs", None),
        P("fs", None),
    )
    return jax.shard_map(
        on_device,
        mesh=mesh,
        in_specs=placed,
        out_specs=(
            P("tp", None, None),
            P("tp", None, None),
            P("tp", None, None),
            P(None, "tp"),
            P(None, "tp"),
            P(None, "tp"),
            P("fs", "tp"),
        ),
        check_vma=False,
    )
```

time: 308 us -> 120 us (0.39)
  the two profiles are of different devices: /device:TPU:1 before, /device:TPU:16 now
where the time goes in v1:
time: 120 us; the launch traced here: 119 us
  Pallas kernels  96.6 us (80%)
  local copies, waits for them, and re-layouts  22.2 us (18%)
    pallas_call x1, Pallas kernels, on_device(): pl.pallas_call(functools.partial(kernel, n_tp, nz, units, cap), name='han...  96.6 us
    unnamed x16, local copies, waits for them, and re-layouts  22.2 us

profile of v1, /device:TPU:16, one launch (start us, length us, event | category | flops | bytes accessed | tf_op | source)
XLA Modules:
  0.0 119.4 jit_solution(6291783780493864514)
XLA Ops:
  0.6 1.5 %copy.20.ids = s32[256,8]{1,0:T(8,128)} copy(s32[256,8]{0,1:T(8,128)} %param.18) | data formatting | bytes 16384 | tf_op args[8]
  2.1 1.5 %copy.21.scores = f32[256,8]{1,0:T(8,128)} copy(f32[256,8]{0,1:T(8,128)} %param.19) | data formatting | bytes 16384 | tf_op args[9]
  3.6 1.9 %copy.17.tg = f32[32,21,64]{2,1,0:T(8,128)} copy(f32[32,21,64]{2,0,1:T(8,128)} %param.10) | data formatting | bytes 344064 | tf_op args[0]
  5.5 1.9 %copy.18.tu = f32[32,21,64]{2,1,0:T(8,128)} copy(f32[32,21,64]{2,0,1:T(8,128)} %param.11) | data formatting | bytes 344064 | tf_op args[1]
  7.5 1.9 %copy.19.td = f32[32,21,64]{2,1,0:T(8,128)} copy(f32[32,21,64]{2,0,1:T(8,128)} %param.12) | data formatting | bytes 344064 | tf_op args[2]
  9.4 96.6 %hand_over.1 = (bf16[3,168,2048]{2,1,0:T(8,128)(2,1)}, bf16[3,168,2048]{2,1,0:T(8,128)(2,1)}, bf16[3,168,2048]{2,1,0:T(8,128)(2,1)}, bf16[504,64]{1,0:T(8,128)(2...) custom-call(f32[32,21,64]{2,1,0:T(8,128)} %copy.17.tg, f32[32,21,64]{2,1,0:T(8,128)} %copy.18.tu, ...), custom_call_target="tpu_custom_call" | custom-call | tf_op jit(solution)/shard_map/hand_over/pallas_call | solution.py:461
  106.0 1.5 %copy.25 = bf16[256,64]{0,1:T(8,128)(2,1)} copy(bf16[256,64]{1,0:T(8,128)(2,1)} %get-tuple-element.27) | data formatting | bytes 65536
  107.5 1.7 %copy.22 = bf16[504,64]{0,1:T(8,128)(2,1)} copy(bf16[504,64]{1,0:T(8,128)(2,1)} %get-tuple-element.24) | data formatting | bytes 129024
  109.2 1.7 %copy.23 = bf16[504,64]{0,1:T(8,128)(2,1)} copy(bf16[504,64]{1,0:T(8,128)(2,1)} %get-tuple-element.25) | data formatting | bytes 129024
  110.8 1.7 %copy.24 = bf16[504,64]{0,1:T(8,128)(2,1)} copy(bf16[504,64]{1,0:T(8,128)(2,1)} %get-tuple-element.26) | data formatting | bytes 129024
  112.5 0.0 copy-start.1
  112.5 3.3 %copy.29 = bf16[1,504,2048]{2,1,0:T(8,128)(2,1)} copy(bf16[1,504,2048]{2,1,0:T(8,128)(2,1)} %bitcast.6) | data formatting | bytes 4128768
  115.7 0.0 copy-done.1
  115.8 0.0 copy-start
  115.8 1.3 %copy.30 = bf16[1,504,2048]{2,1,0:T(8,128)(2,1)} copy(bf16[1,504,2048]{2,1,0:T(8,128)(2,1)S(1)} %bitcast.5) | data formatting | bytes 4128768
  117.1 1.0 copy-done
  118.1 1.3 %copy.31 = bf16[1,504,2048]{2,1,0:T(8,128)(2,1)} copy(bf16[1,504,2048]{2,1,0:T(8,128)(2,1)S(1)} %bitcast.4) | data formatting | bytes 4128768
Async XLA Ops:
  112.5 3.3 %copy-start.1 = (bf16[3,168,2048]{2,1,0:T(8,128)(2,1)S(1)}, bf16[3,168,2048]{2,1,0:T(8,128)(2,1)}, u32[]{:S(2)}) copy-start(bf16[3,168,2048]{2,1,0:T(8,128)(2,1)} %get-tuple-element.15) | copy-start | bytes 6193156
  115.8 2.3 %copy-start = (bf16[3,168,2048]{2,1,0:T(8,128)(2,1)S(1)}, bf16[3,168,2048]{2,1,0:T(8,128)(2,1)}, u32[]{:S(2)}) copy-start(bf16[3,168,2048]{2,1,0:T(8,128)(2,1)} %get-tuple-element.16) | copy-start | bytes 6193156

commit v2 on v1

--- a/solution.py
+++ b/solution.py
@@ -49,11 +49,10 @@
     n_tp, nz, units, cap,
     tg, tu, td, sg, su, sd, gain, tok, ids, scores,
     o_gate, o_up, o_down, o_sgate, o_sup, o_sdown, o_mix,
-    send_a, recv_a, blocks, small, normed, rows, total, spread, slot_weight,
-    pre_send, pre_recv, acts, sdown, send_x, recv_x, send_y, recv_y, staged,
+    packed, send_a, recv_a, blocks, small, normed, rows, total, spread, slot_weight,
+    pre_send, pre_recv, acts, sdown, send_x, recv_x, send_y, recv_y,
     sem_a, sem_ring_s, sem_ring_r, sem_pair_s, sem_pair_r,
     sem_small_s, sem_small_r, sem_spair, sem_j, sem_act, sem_x_s, sem_x_r, sem_y_s, sem_y_r,
-    sem_out,
 ):
     n_y = n_tp // NX
     far = nz // 2
@@ -82,20 +81,30 @@
         pl.semaphore_signal(barrier, inc=1, device_id={"fs": other}, device_id_type=MESH)
     lax.fori_loop(1, n_tp, greet, 0)
 
-    def pack(g, u, d):
-        stack = jnp.concatenate([g, u, d, jnp.zeros((ROW - 3 * units, 64), F32)], axis=0)
-        return jnp.concatenate([stack[: ROW // 2], stack[ROW // 2 :]], axis=1).astype(BF16)
-
     scale = gain[...]
 
-    def prepare(e, _):
-        send_a[e] = pack(tg[e] * scale, tu[e] * scale, td[e])
-        return 0
-
-    small[z, core] = pack(sg[...] * scale, su[...] * scale, sd[...])
-    lax.fori_loop(0, n_tp, prepare, 0)
-    recv_a[me] = send_a[me]
-    pl.semaphore_wait(barrier, n_tp + 2)
+    with jax.named_scope("pack"):
+
+        def unit(r):
+            if r < units:
+                return tg[r] * scale
+            if r < 2 * units:
+                return tu[r - units] * scale
+            return td[r - 2 * units] if r < 3 * units else jnp.zeros((n_tp, 64), F32)
+
+        parts = [sg[...] * scale, su[...] * scale, sd[...]]
+        stack = jnp.concatenate([*parts, jnp.zeros((ROW - 3 * units, 64), F32)], axis=0)
+        stack = jnp.concatenate([stack[: ROW // 2], stack[ROW // 2 :]], axis=1)
+        small[z, core] = stack.astype(BF16)
+        for r in range(0, ROW // 2, 8):
+            several = [
+                jnp.concatenate([unit(i), unit(i + ROW // 2)], axis=1) for i in range(r, r + 8)
+            ]
+            packed[:, pl.ds(r, 8), :] = jnp.swapaxes(jnp.stack(several, axis=0), 0, 1)
+        send_a[...] = packed[...].astype(BF16)
+        recv_a[me] = send_a[me]
+    with jax.named_scope("entry"):
+        pl.semaphore_wait(barrier, n_tp + 2)
 
     def plane(src, dst, sems, peer):
         return pltpu.make_async_remote_copy(
@@ -159,20 +168,19 @@
         tf * lax.rsqrt(jnp.mean(tf * tf, axis=1, keepdims=True) + EPSILON)
     ).astype(BF16)
     ids_v, sc = ids[...], scores[...]
-    ratio = ROUTED_SCALE * sc / jnp.sum(sc, axis=1, keepdims=True)
+    ratio = ROUTED_SCALE * sc / jnp.sum(sc, axis=0, keepdims=True)
+    expert_row = iota((128, tokens), 0)
+    present = jnp.zeros((128, tokens), F32)
+    weight_row = jnp.zeros((1, tokens), F32)
+    for k in range(ids.shape[0]):
+        present = jnp.where(ids_v[k : k + 1] == expert_row, 1.0, present)
+        weight_row += jnp.where(ids_v[k : k + 1] == me, ratio[k : k + 1], 0.0)
+    before = jnp.where(iota((tokens, tokens), 0) < iota((tokens, tokens), 1), 1.0, 0.0)
+    position = nn(present.astype(BF16), before.astype(BF16))
+    slots = jnp.where(present > 0.0, position, -1.0)
+    slot_row = jnp.sum(jnp.where(expert_row == me, slots, 0.0), axis=0, keepdims=True)
+    slot = slots.T
     lane = iota((tokens, 128), 1)
-    present = jnp.zeros((tokens, 128), F32)
-    weight = jnp.zeros((tokens, 128), F32)
-    for k in range(ids.shape[1]):
-        hit = ids_v[:, k : k + 1] == lane
-        present = jnp.where(hit, 1.0, present)
-        weight = jnp.where(hit, weight + ratio[:, k : k + 1], weight)
-    before = jnp.where(iota((tokens, tokens), 1) < iota((tokens, tokens), 0), 1.0, 0.0)
-    position = nn(before.astype(BF16), present.astype(BF16))
-    slot = jnp.where(present > 0.0, position, -1.0)
-    mine = iota((128, tokens), 0) == me
-    slot_row = jnp.sum(jnp.where(mine, slot.T, 0.0), axis=0, keepdims=True)
-    weight_row = jnp.sum(jnp.where(mine, weight.T, 0.0), axis=0, keepdims=True)
     taken = slot_row == iota((cap, tokens), 0).astype(F32)
     slot_weight[...] = jnp.broadcast_to(
         jnp.sum(jnp.where(taken, weight_row, 0.0), axis=1, keepdims=True), slot_weight.shape
@@ -235,11 +243,11 @@
             for m in range(3)
         ]
 
+    def padded(v):
+        spare = jnp.zeros((-hidden % 128, 128), F32)
+        return jnp.concatenate([v, spare], axis=0)
+
     def shared_rows():
-        def spent(i, _):
-            small_pair(z).wait_recv()
-            return 0
-
         got = [[], [], []]
         for g in range(groups):
             v = small[pl.ds(4 * g, 4)].reshape(8, ROW // 2, 128).astype(F32)
@@ -249,7 +257,7 @@
                 got[m].append(nn(p, v))
         gate, up, down = [jnp.concatenate(one, axis=0) for one in got]
         for o, v in ((o_sgate, gate), (o_sup, up), (o_sdown, down)):
-            o[...] = v[:, :64].astype(BF16)
+            o[...] = padded(v).T[:64, :hidden].astype(BF16)
         pad = jnp.zeros((n_tp * per_j - hidden, 128), F32)
         both = jnp.concatenate([halves(gate, up)[0], pad], axis=0)
         pre_send[...] = both.astype(BF16).reshape(n_tp, per_j, 128)
@@ -357,20 +365,16 @@
     steps = width // part
     outs = (o_gate, o_up, o_down)
 
-    def leave(m, g):
-        return pltpu.make_async_copy(staged.at[m, g], outs[m].at[g], sem_out.at[m, g])
-
     for g in range(groups):
         for m, p in enumerate(picks()):
 
             def served(n, _, m=m, g=g, p=p):
                 cols = pl.ds(pl.multiple_of(n * part, part), part)
                 v = blocks[pl.ds(4 * g, 4), :, :, cols].reshape(8 * ROW, part)
-                staged[m, g, :, cols] = nn(p, v).astype(BF16)
+                outs[m][g, :, cols] = nn(p, v).astype(BF16)
                 return 0
 
             lax.fori_loop(0, steps, served, 0)
-            leave(m, g).start()
 
     for i in range(1, NX):
         row_copy(i).wait_send()
@@ -411,8 +415,8 @@
         col_copy(i).wait_recv()
     for i in range(n_y):
         mixed += recv_y[i].astype(F32)
-    upper = pltpu.roll(mixed, 64, 1)
-    o_mix[...] = jnp.concatenate([mixed[:, :64], upper[:, :64]], axis=0).astype(BF16)
+    mixed = mixed.T
+    o_mix[...] = jnp.concatenate([mixed[:64], mixed[64:]], axis=1).astype(BF16)
 
     for d in (0, 1):
         for q in range(CHUNKS):
@@ -434,37 +438,45 @@
         return 0
 
     lax.fori_loop(0, nz, pair_sent, 0)
-    for g in range(groups):
-        for m in range(3):
-            leave(m, g).wait()
+
+
+def deliver(*refs):
+    n = (len(refs) - 1) // 2
+    copies = [pltpu.make_async_copy(refs[i], refs[n + i], refs[-1].at[i]) for i in range(n)]
+    for copy in copies:
+        copy.start()
+    for copy in copies:
+        copy.wait()
 
 
 def on_device(*args):
-    tg, ids = args[0], args[8]
-    n_tp, units = tg.shape[0], tg.shape[1]
+    n_tp, units = args[0].shape[:2]
     nz = lax.axis_size("fs") // 2
     tokens, width = args[7].shape
-    top = ids.shape[1]
+    top = args[8].shape[1]
     cap = min(tokens, 5 * tokens * top // (2 * n_tp))
     hidden = nz * 2 * units
     per_j = -(-hidden // (16 * n_tp)) * 16
     n_y = n_tp // NX
     far = nz // 2
     groups = nz // 4
-    args = list(args)
+    args = [jnp.swapaxes(v, 0, 1) for v in args[:3]] + list(args[3:])
     args[6] = args[6].reshape(1, -1)
+    args[8:] = [v.T for v in args[8:]]
     vm = pl.BlockSpec(memory_space=pltpu.VMEM)
     hbm = pl.BlockSpec(memory_space=pl.ANY)
     dma = pltpu.SemaphoreType.DMA
-    big = jax.ShapeDtypeStruct((groups, 8 * units, width), BF16)
-    thin = jax.ShapeDtypeStruct((hidden, 64), BF16)
+    big = pltpu.VMEM((groups, 8 * units, width), BF16)
+    thin = pltpu.VMEM((64, hidden), BF16)
+    mix = pltpu.VMEM((64, tokens), BF16)
     outs = pl.pallas_call(
         functools.partial(kernel, n_tp, nz, units, cap),
         name="hand_over",
-        out_shape=[big, big, big, thin, thin, thin, jax.ShapeDtypeStruct((tokens, 64), BF16)],
+        out_shape=[big, big, big, thin, thin, thin, mix],
         in_specs=[vm] * 10,
-        out_specs=[hbm] * 3 + [vm] * 4,
+        out_specs=[vm] * 7,
         scratch_shapes=[
+            pltpu.VMEM((n_tp, ROW // 2, 128), F32),
             pltpu.VMEM((n_tp, ROW // 2, 128), BF16),
             pltpu.VMEM((n_tp, ROW // 2, 128), BF16),
             pltpu.VMEM((nz, 2, ROW, width), BF16),
@@ -482,7 +494,6 @@
             pltpu.VMEM((NX, cap, 64 * n_y), BF16),
             pltpu.VMEM((n_y, tokens // 2, 128), BF16),
             pltpu.VMEM((n_y, tokens // 2, 128), BF16),
-            pltpu.VMEM((3, groups, 8 * units, width), BF16),
             dma((2,)),
             dma((2, far + 1, CHUNKS)),
             dma((2, far + 1, CHUNKS)),
@@ -497,15 +508,22 @@
             dma((NX,)),
             dma((n_y,)),
             dma((n_y,)),
-            dma((3, groups)),
         ],
         compiler_params=pltpu.CompilerParams(
             collective_id=0, has_side_effects=True, vmem_limit_bytes=56 * 1024 * 1024
         ),
     )(*args)
-    gate, up, down, sgate, sup, sdown, mixture = outs
-    full = [v.reshape(1, hidden, width) for v in (gate, up, down)]
-    return (*full, sgate, sup, sdown, mixture)
+    outs = pl.pallas_call(
+        deliver,
+        name="deliver",
+        out_shape=[jax.ShapeDtypeStruct(v.shape, v.dtype) for v in outs],
+        in_specs=[vm] * 7,
+        out_specs=[hbm] * 7,
+        scratch_shapes=[dma((7,))],
+        compiler_params=pltpu.CompilerParams(vmem_limit_bytes=1024 * 1024),
+    )(*[pltpu.with_memory_space_constraint(v, pltpu.VMEM) for v in outs])
+    full = [v.reshape(1, hidden, width) for v in outs[:3]]
+    return (*full, *[v.T for v in outs[3:]])
 
 
 def solution(mesh):

time: 120 us -> 99.4 us (0.83)
  local copies, waits for them, and re-layouts: 22.2 us -> 0 us
  Pallas kernels: 96.6 us -> 98.6 us
    unnamed x16 -> x0, local copies, waits for them, and re-layouts: 22.2 us -> none
    pallas_call x0 -> x1, Pallas kernels: none -> 2.78 us  [on_device(): pl.pallas_call(deliver, name='deliver', out_shape=[jax.ShapeDtypeStruct(v...]
where the time goes in v2:
time: 99.4 us; the launch traced here: 99.3 us
  Pallas kernels  98.6 us (99%)
    pallas_call x1, Pallas kernels, on_device(): pl.pallas_call(functools.partial(kernel, n_tp, nz, units, cap), name='han...  95.9 us
    pallas_call x1, Pallas kernels, on_device(): pl.pallas_call(deliver, name='deliver', out_shape=[jax.ShapeDtypeStruct(v...  2.78 us

profile of v2, /device:TPU:16, one launch (start us, length us, event | category | flops | bytes accessed | tf_op | source)
XLA Modules:
  0.0 99.3 jit_solution(17561215184601453649)
XLA Ops:
  0.6 95.9 %hand_over.1 = (bf16[3,168,2048]{2,1,0:T(8,128)(2,1)S(1)}, bf16[3,168,2048]{2,1,0:T(8,128)(2,1)S(1)}, bf16[3,168,2048]{2,1,0:T(8,128)(2,1)S(1)}, bf16[64,504]{1,...) custom-call(f32[21,32,64]{2,1,0:T(8,128)} %bitcast.13, ...), custom_call_target="tpu_custom_call" | custom-call | tf_op jit(solution)/shard_map/hand_over/pallas_call | solution.py:472
  96.5 2.8 %deliver.1 = (bf16[3,168,2048]{2,1,0:T(8,128)(2,1)}, bf16[3,168,2048]{2,1,0:T(8,128)(2,1)}, bf16[3,168,2048]{2,1,0:T(8,128)(2,1)}, bf16[64,504]{1,0:T(8,128)(2,1...) custom-call(bf16[3,168,2048]{2,1,0:T(8,128)(2,1)S(1)} %get-tuple-element.21.refs_0_, ...), custom_call_target="tpu_custom_call" | custom-call | tf_op jit(solution)/shard_map/deliver/pallas_call | solution.py:516

commit v3 on v2

--- a/solution.py
+++ b/solution.py
@@ -11,8 +11,9 @@
 ROUTED_SCALE = 2.5
 MESH = pl.DeviceIdType.MESH
 NX = 4
-CHUNKS = 4
 ROW = 64
+PIECE = 16
+ORDER = (0, 2, 1, 3)
 F32, BF16 = jnp.float32, jnp.bfloat16
 
 
@@ -47,11 +48,21 @@
 
 def kernel(
     n_tp, nz, units, cap,
+    *refs,
+):
+    hbm_in, refs = refs[:10], refs[10:]
+    outs, refs = refs[:7], refs[7:]
+    inputs, refs = refs[:10], refs[10:]
+    body(n_tp, nz, units, cap, hbm_in, *inputs, *outs, *refs)
+
+
+def body(
+    n_tp, nz, units, cap, hbm_in,
     tg, tu, td, sg, su, sd, gain, tok, ids, scores,
     o_gate, o_up, o_down, o_sgate, o_sup, o_sdown, o_mix,
-    packed, send_a, recv_a, blocks, small, normed, rows, total, spread, slot_weight,
+    packed, pick, send_a, recv_a, blocks, small, normed, rows, total, spread, slot_weight,
     pre_send, pre_recv, acts, sdown, send_x, recv_x, send_y, recv_y,
-    sem_a, sem_ring_s, sem_ring_r, sem_pair_s, sem_pair_r,
+    sem_in, sem_a, sem_ring_s, sem_ring_r, sem_pair_s, sem_pair_r,
     sem_small_s, sem_small_r, sem_spair, sem_j, sem_act, sem_x_s, sem_x_r, sem_y_s, sem_y_r,
 ):
     n_y = n_tp // NX
@@ -80,6 +91,12 @@
     for other in (ahead, behind, twin):
         pl.semaphore_signal(barrier, inc=1, device_id={"fs": other}, device_id_type=MESH)
     lax.fori_loop(1, n_tp, greet, 0)
+    vmem_in = (tg, tu, td, sg, su, sd, gain, tok, ids, scores)
+    loads = [pltpu.make_async_copy(hbm_in[i], vmem_in[i], sem_in.at[i]) for i in range(10)]
+    for load in loads:
+        load.start()
+    for i in (0, 1, 2, 3, 4, 5, 6):
+        loads[i].wait()
 
     scale = gain[...]
 
@@ -101,20 +118,21 @@
                 jnp.concatenate([unit(i), unit(i + ROW // 2)], axis=1) for i in range(r, r + 8)
             ]
             packed[:, pl.ds(r, 8), :] = jnp.swapaxes(jnp.stack(several, axis=0), 0, 1)
-        send_a[...] = packed[...].astype(BF16)
-        recv_a[me] = send_a[me]
+        for h in (0, 1):
+            send_a[h] = packed[:, pl.ds(PIECE * h, PIECE), :].astype(BF16)
+            recv_a[h, me] = send_a[h, me]
     with jax.named_scope("entry"):
         pl.semaphore_wait(barrier, n_tp + 2)
 
-    def plane(src, dst, sems, peer):
-        return pltpu.make_async_remote_copy(
-            src_ref=src, dst_ref=dst, send_sem=sems.at[0], recv_sem=sems.at[1],
+    def plane(src, dst, sems, peer, at=0):
+        return pltpu.make_async_remote_copy(
+            src_ref=src, dst_ref=dst, send_sem=sems.at[at], recv_sem=sems.at[at + 1],
             device_id={"tp": peer}, device_id_type=MESH,
         )
 
-    def plane_done(ref, sems):
+    def plane_done(ref, sems, at=0):
         piece = ref.at[pl.ds(0, n_tp - 1)]
-        done = plane(piece, piece, sems, lax.rem(me + 1, n_tp))
+        done = plane(piece, piece, sems, lax.rem(me + 1, n_tp), at)
         done.wait_send()
         done.wait_recv()
 
@@ -139,12 +157,14 @@
     small_hop(1, 1, z).start()
     small_pair(z).start()
 
-    def send_weights(i, _):
-        peer = lax.rem(me + i, n_tp)
-        plane(send_a.at[peer], recv_a.at[me], sem_a, peer).start()
-        return 0
-
-    lax.fori_loop(1, n_tp, send_weights, 0)
+    for h in (0, 1):
+
+        def send_weights(i, _, h=h):
+            peer = lax.rem(me + i, n_tp)
+            plane(send_a.at[h, peer], recv_a.at[h, me], sem_a, peer, 2 * h).start()
+            return 0
+
+        lax.fori_loop(1, n_tp, send_weights, 0)
 
     def small_step(s):
         for d in (0, 1):
@@ -163,6 +183,8 @@
             else:
                 pl.when(s < far)(arrived)
 
+    for i in (7, 8, 9):
+        loads[i].wait()
     tf = tok[...].astype(F32)
     normed[...] = (
         tf * lax.rsqrt(jnp.mean(tf * tf, axis=1, keepdims=True) + EPSILON)
@@ -191,18 +213,16 @@
         spread[i] = jnp.where(col == iota((tokens, cap), 1).astype(F32), 1.0, 0.0).astype(BF16)
     total[...] = jnp.zeros_like(total)
 
-    small_step(1)
-    plane_done(recv_a, sem_a)
-
-    for m in range(n_tp // 2):
-        top, low = halves(recv_a[2 * m].astype(F32), recv_a[2 * m + 1].astype(F32))
-        whole = jnp.concatenate([top, low], axis=0)
-        blocks[z, core, :, pl.ds(128 * m, 128)] = whole.astype(BF16)
-
-    size = ROW // CHUNKS
+    shape = (group_rows, 8 * ROW)
+    i, f, r = iota(shape, 0), iota(shape, 1) // ROW, iota(shape, 1) & (ROW - 1)
+    ordered = []
+    for m in range(3):
+        inside = (r >= units * m) & (r < units * (m + 1))
+        ordered.append(jnp.where(inside & (i == units * f + r - units * m), 1.0, 0.0))
+    pick[...] = jnp.concatenate(ordered, axis=0).astype(BF16)
 
     def hop(d, s, q, at):
-        piece = blocks.at[at, core, pl.ds(q * size, size)]
+        piece = blocks.at[at, core, pl.ds(q * PIECE, PIECE)]
         return pltpu.make_async_remote_copy(
             src_ref=piece, dst_ref=piece,
             send_sem=sem_ring_s.at[d, s, q], recv_sem=sem_ring_r.at[d, s, q],
@@ -217,31 +237,38 @@
             device_id={"fs": twin}, device_id_type=MESH,
         )
 
-    for q in range(CHUNKS):
-        for d in (0, 1):
-            hop(d, 1, q, z).start()
+    early = far // 2
+    with jax.named_scope("small_early"):
+        for i in range(1, early + 1):
+            small_step(i)
+    for h in (0, 1):
+        with jax.named_scope(f"await_weights{h}"):
+            plane_done(recv_a.at[h], sem_a, 2 * h)
+        with jax.named_scope("unpack"):
+            for m in range(n_tp // 2):
+                upper, lower = recv_a[h, 2 * m].astype(F32), recv_a[h, 2 * m + 1].astype(F32)
+                for part, v in enumerate(halves(upper, lower)):
+                    at = pl.ds(PIECE * (h + 2 * part), PIECE)
+                    blocks[z, core, at, pl.ds(128 * m, 128)] = v.astype(BF16)
+        for q in ORDER[2 * h : 2 * h + 2]:
+            for d in (0, 1):
+                hop(d, 1, q, z).start()
     pair(z).start()
 
     def last_leg(d, q):
-        return (q < CHUNKS // 2) == (d == 0)
-
-    def expert(at):
-        pair(at).wait_recv()
-        w = blocks[at].reshape(2 * ROW, width)
-        pre = nt(rows[...], w)
+        return (q in ORDER[:2]) == (d == 0)
+
+    def activated(at):
+        with jax.named_scope("await_pair"):
+            pair(at).wait_recv()
+        pre = nt(rows[...], blocks[at].reshape(2 * ROW, width))
         act = silu(pltpu.roll(pre, 2 * units, 1)) * pltpu.roll(pre, units, 1)
         unit = iota(act.shape, 1) & (ROW - 1)
-        act = jnp.where((unit >= 2 * units) & (unit < 3 * units), act, 0.0).astype(BF16)
-        total[...] += nn(act, w)
-
-    def picks():
-        shape = (group_rows, 8 * ROW)
-        i, c = iota(shape, 0), iota(shape, 1)
-        f, r = c // ROW, c & (ROW - 1)
-        return [
-            jnp.where((r >= units * m) & (r < units * (m + 1)) & (i == units * f + r - units * m), 1.0, 0.0).astype(BF16)
-            for m in range(3)
-        ]
+        return jnp.where((unit >= 2 * units) & (unit < 3 * units), act, 0.0).astype(BF16)
+
+    def expert(at):
+        act = activated(at)
+        total[...] += nn(act, blocks[at].reshape(2 * ROW, width))
 
     def padded(v):
         spare = jnp.zeros((-hidden % 128, 128), F32)
@@ -253,8 +280,9 @@
             v = small[pl.ds(4 * g, 4)].reshape(8, ROW // 2, 128).astype(F32)
             v = jnp.concatenate([v, pltpu.roll(v, 64, 2)], axis=1).reshape(8 * ROW, 128)
             v = v.astype(BF16)
-            for m, p in enumerate(picks()):
-                got[m].append(nn(p, v))
+            found = nn(pick[...], v)
+            for m in range(3):
+                got[m].append(found[group_rows * m : group_rows * (m + 1)])
         gate, up, down = [jnp.concatenate(one, axis=0) for one in got]
         for o, v in ((o_sgate, gate), (o_sup, up), (o_sdown, down)):
             o[...] = padded(v).T[:64, :hidden].astype(BF16)
@@ -273,40 +301,58 @@
 
         lax.fori_loop(1, n_tp, send, 0)
 
+    def shared_acts():
+        with jax.named_scope("await_j"):
+            plane_done(pre_recv, sem_j)
+        gates, ups = [], []
+        for m in range(n_tp // 2):
+            g, u = halves(pre_recv[2 * m].astype(F32), pre_recv[2 * m + 1].astype(F32))
+            gates.append(g.astype(BF16))
+            ups.append(u.astype(BF16))
+        gate = nt(jnp.concatenate(gates, axis=1), normed[...])
+        up = nt(jnp.concatenate(ups, axis=1), normed[...])
+        acts[me] = (silu(gate) * up).astype(BF16)
+
+        def send_act(i, _):
+            peer = lax.rem(me + i, n_tp)
+            plane(acts.at[me], acts.at[me], sem_act, peer).start()
+            return 0
+
+        lax.fori_loop(1, n_tp, send_act, 0)
+
     def ring_step(s, _):
-        for q in range(CHUNKS):
+        for n, q in enumerate(ORDER):
             for d in (0, 1):
-
-                def arrived(d=d, q=q):
-                    at = origin(d, s)
+                at = origin(d, s)
+                with jax.named_scope(f"arrive{d}{n}"):
                     hop(d, s, q, at).wait_recv()
-                    go = s + 1 <= far if last_leg(d, q) else s + 1 < far
-
-                    @pl.when(go)
-                    def _():
+                if last_leg(d, q):
+                    hop(d, s + 1, q, at).start()
+                else:
+
+                    @pl.when(s + 1 < far)
+                    def _(d=d, q=q, at=at):
                         hop(d, s + 1, q, at).start()
 
-                if last_leg(d, q):
-                    arrived()
-                else:
-                    pl.when(s < far)(arrived)
-        pair(origin(0, s)).start()
-
-        @pl.when(s < far)
+            if n == 1:
+                with jax.named_scope("expert0"):
+                    expert(origin(0, s - 1))
+            if n == 2:
+
+                @pl.when(s > 1)
+                def _():
+                    with jax.named_scope("expert1"):
+                        expert(origin(1, s - 1))
+
+        for d in (0, 1):
+            pair(origin(d, s)).start()
+
+        @pl.when(s + early <= far)
         def _():
-            pair(origin(1, s)).start()
-
-        @pl.when(s < far)
-        def _():
-            small_step(s + 1)
-
-        def one(i, _):
-            expert(lax.rem(z + nz + (s - 1) * (1 - 2 * i), nz))
-            return 0
-
-        lax.fori_loop(0, jnp.where(s == 1, 1, 2), one, 0)
-
-        @pl.when(s == far)
+            with jax.named_scope("small"):
+                small_step(s + early)
+
+        @pl.when(s == far - early)
         def _():
             everything = small.at[:, 0]
             done = pltpu.make_async_remote_copy(
@@ -316,110 +362,125 @@
             )
             done.wait_send()
             done.wait_recv()
-            shared_rows()
+            with jax.named_scope("shared_rows"):
+                shared_rows()
+
+        @pl.when(s == far - early + 1)
+        def _():
+            with jax.named_scope("shared_acts"):
+                shared_acts()
 
         return 0
 
-    lax.fori_loop(1, far + 1, ring_step, 0)
-    expert(lax.rem(z + far, nz))
+    lax.fori_loop(1, far, ring_step, 0)
+    for d in (0, 1):
+        with jax.named_scope("expert_near_last"):
+            expert(origin(d, far - 1))
+    opposite = lax.rem(z + far, nz)
+    with jax.named_scope("arrive_last"):
+        for q in ORDER:
+            hop(0 if q in ORDER[:2] else 1, far, q, opposite).wait_recv()
+    pair(opposite).start()
+    with jax.named_scope("expert_last"):
+        act = activated(opposite)
 
     w = slot_weight[...]
-    for p in range(n_y // 2):
+    pairs = n_y // 2
+    turns = [(pairs // 2 + (i + 1) // 2 * (1 if i % 2 else -1)) % pairs for i in range(pairs)]
+    turns = [i for i in turns if i] + [0]
+
+    def quarter(k):
+        return lax.rem(y // 2 + turns[k], pairs)
+
+    def row_copy(k, i):
+        to = lax.rem(x + i, NX)
+        return pltpu.make_async_remote_copy(
+            src_ref=send_x.at[to, k], dst_ref=recv_x.at[x, k],
+            send_sem=sem_x_s.at[k, i], recv_sem=sem_x_r.at[k, i],
+            device_id={"tp": y * NX + to}, device_id_type=MESH,
+        )
+
+    for k in range(pairs):
+        p = quarter(k)
         for h in range(NX // 2):
-            a = total[:, pl.ds(128 * (2 * p * (NX // 2) + h), 128)] * w
-            b = total[:, pl.ds(128 * ((2 * p + 1) * (NX // 2) + h), 128)] * w
-            left, right = halves(a, b)
-            send_x[2 * h, :, pl.ds(128 * p, 128)] = left.astype(BF16)
-            send_x[2 * h + 1, :, pl.ds(128 * p, 128)] = right.astype(BF16)
-
-    def row_copy(i):
-        to = lax.rem(x + i, NX)
-        return pltpu.make_async_remote_copy(
-            src_ref=send_x.at[to], dst_ref=recv_x.at[x],
-            send_sem=sem_x_s.at[i], recv_sem=sem_x_r.at[i],
-            device_id={"tp": y * NX + to}, device_id_type=MESH,
-        )
-
-    for i in range(1, NX):
-        row_copy(i).start()
-    recv_x[x] = send_x[x]
-
-    plane_done(pre_recv, sem_j)
-    gates, ups = [], []
-    for m in range(n_tp // 2):
-        g, u = halves(pre_recv[2 * m].astype(F32), pre_recv[2 * m + 1].astype(F32))
-        gates.append(g.astype(BF16))
-        ups.append(u.astype(BF16))
-    gate = nt(jnp.concatenate(gates, axis=1), normed[...])
-    up = nt(jnp.concatenate(ups, axis=1), normed[...])
-    acts[me] = (silu(gate) * up).astype(BF16)
-
-    def send_act(i, _):
-        peer = lax.rem(me + i, n_tp)
-        plane(acts.at[me], acts.at[me], sem_act, peer).start()
-        return 0
-
-    lax.fori_loop(1, n_tp, send_act, 0)
+            several = []
+            for i in (2 * p, 2 * p + 1):
+                cols = pl.ds(pl.multiple_of(128 * (i * (NX // 2) + h), 128), 128)
+                new = nn(act, blocks[opposite, :, :, cols].reshape(2 * ROW, 128))
+                several.append((total[:, cols] + new) * w)
+            for i, v in enumerate(halves(*several)):
+                send_x[2 * h + i, k] = v.astype(BF16)
+        for i in (2, 1, 3) if NX == 4 else range(1, NX):
+            row_copy(k, i).start()
+        recv_x[x, k] = send_x[x, k]
 
     part = min(512, width)
-    steps = width // part
-    outs = (o_gate, o_up, o_down)
-
-    for g in range(groups):
-        for m, p in enumerate(picks()):
-
-            def served(n, _, m=m, g=g, p=p):
-                cols = pl.ds(pl.multiple_of(n * part, part), part)
-                v = blocks[pl.ds(4 * g, 4), :, :, cols].reshape(8 * ROW, part)
-                outs[m][g, :, cols] = nn(p, v).astype(BF16)
-                return 0
-
-            lax.fori_loop(0, steps, served, 0)
-
-    for i in range(1, NX):
-        row_copy(i).wait_send()
-        row_copy(i).wait_recv()
+    results = (o_gate, o_up, o_down)
+
+    def served(g):
+        def some(n, _):
+            cols = pl.ds(pl.multiple_of(n * part, part), part)
+            v = blocks[pl.ds(4 * g, 4), :, :, cols].reshape(8 * ROW, part)
+            v = nn(pick[...], v)
+            for m in range(3):
+                results[m][g, :, cols] = v[group_rows * m : group_rows * (m + 1)].astype(BF16)
+            return 0
+
+        with jax.named_scope("served"):
+            lax.fori_loop(0, width // part, some, 0)
+
+    for g in range(groups - 1):
+        served(g)
 
     half = tokens // 2
-    for p in range(n_y // 2):
+    odd = lax.rem(y, 2)
+
+    def col_copy(k, h):
+        last = k == pairs - 1
+        to = 2 * quarter(k) + (1 - odd if last else h)
+        return pltpu.make_async_remote_copy(
+            src_ref=send_y.at[to], dst_ref=recv_y.at[y],
+            send_sem=sem_y_s.at[k, h], recv_sem=sem_y_r.at[k, 0 if last else odd],
+            device_id={"tp": to * NX + x}, device_id_type=MESH,
+        )
+
+    def col_arrival(k, h):
+        return pltpu.make_async_remote_copy(
+            src_ref=recv_y.at[0], dst_ref=recv_y.at[0],
+            send_sem=sem_y_s.at[k, h], recv_sem=sem_y_r.at[k, h],
+            device_id={"tp": lax.rem(me + 1, n_tp)}, device_id_type=MESH,
+        )
+
+    y_copies = [(k, h) for k in range(pairs) for h in (0, 1) if k < pairs - 1 or h == 0]
+    for k in range(pairs):
+        with jax.named_scope(f"await_x{k}"):
+            for i in range(1, NX):
+                row_copy(k, i).wait_recv()
         acc = jnp.zeros((tokens, 128), F32)
         for i in range(NX):
-            acc += nn(spread[i], recv_x[i, :, pl.ds(128 * p, 128)])
-        left, right = halves(acc[:half], acc[half:])
-        send_y[2 * p] = left.astype(BF16)
-        send_y[2 * p + 1] = right.astype(BF16)
-
-    def col_copy(i):
-        to = lax.rem(y + i, n_y)
-        return pltpu.make_async_remote_copy(
-            src_ref=send_y.at[to], dst_ref=recv_y.at[y],
-            send_sem=sem_y_s.at[i], recv_sem=sem_y_r.at[i],
-            device_id={"tp": to * NX + x}, device_id_type=MESH,
-        )
-
-    for i in range(1, n_y):
-        col_copy(i).start()
+            acc += nn(spread[i], recv_x[i, k])
+        for h, v in enumerate(halves(acc[:half], acc[half:])):
+            send_y[2 * quarter(k) + h] = v.astype(BF16)
+        for h in (0, 1):
+            if (k, h) in y_copies:
+                col_copy(k, h).start()
     recv_y[y] = send_y[y]
-
-    def act_done():
-        piece = acts.at[pl.ds(0, n_tp - 1)]
-        done = plane(piece, piece, sem_act, lax.rem(me + 1, n_tp))
-        done.wait_send()
-        done.wait_recv()
-
-    act_done()
+    served(groups - 1)
+
+    with jax.named_scope("await_act"):
+        plane_done(acts, sem_act)
     shared = tn(acts[...].reshape(n_tp * per_j, tokens), sdown[...])
     mixed = halves(shared[:half], shared[half:])[0]
-    for i in range(1, n_y):
-        col_copy(i).wait_send()
-        col_copy(i).wait_recv()
+    with jax.named_scope("await_y"):
+        for k, h in y_copies:
+            col_arrival(k, h).wait_recv()
     for i in range(n_y):
         mixed += recv_y[i].astype(F32)
     mixed = mixed.T
     o_mix[...] = jnp.concatenate([mixed[:64], mixed[64:]], axis=1).astype(BF16)
 
     for d in (0, 1):
-        for q in range(CHUNKS):
+        for q in ORDER:
 
             def sent(s, _, d=d, q=q):
                 hop(d, s, q, z).wait_send()
@@ -438,6 +499,11 @@
         return 0
 
     lax.fori_loop(0, nz, pair_sent, 0)
+    for k in range(pairs):
+        for i in range(1, NX):
+            row_copy(k, i).wait_send()
+    for k, h in y_copies:
+        col_copy(k, h).wait_send()
 
 
 def deliver(*refs):
@@ -473,12 +539,14 @@
         functools.partial(kernel, n_tp, nz, units, cap),
         name="hand_over",
         out_shape=[big, big, big, thin, thin, thin, mix],
-        in_specs=[vm] * 10,
+        in_specs=[hbm] * 10,
         out_specs=[vm] * 7,
         scratch_shapes=[
+            *[pltpu.VMEM(v.shape, v.dtype) for v in args],
             pltpu.VMEM((n_tp, ROW // 2, 128), F32),
-            pltpu.VMEM((n_tp, ROW // 2, 128), BF16),
-            pltpu.VMEM((n_tp, ROW // 2, 128), BF16),
+            pltpu.VMEM((24 * units, 8 * ROW), BF16),
+            pltpu.VMEM((2, n_tp, PIECE, 128), BF16),
+            pltpu.VMEM((2, n_tp, PIECE, 128), BF16),
             pltpu.VMEM((nz, 2, ROW, width), BF16),
             pltpu.VMEM((nz, 2, ROW // 2, 128), BF16),
             pltpu.VMEM((tokens, width), BF16),
@@ -490,13 +558,14 @@
             pltpu.VMEM((n_tp, per_j, 128), BF16),
             pltpu.VMEM((n_tp, per_j, tokens), BF16),
             pltpu.VMEM((n_tp * per_j, 128), BF16),
-            pltpu.VMEM((NX, cap, 64 * n_y), BF16),
-            pltpu.VMEM((NX, cap, 64 * n_y), BF16),
+            pltpu.VMEM((NX, n_y // 2, cap, 128), BF16),
+            pltpu.VMEM((NX, n_y // 2, cap, 128), BF16),
             pltpu.VMEM((n_y, tokens // 2, 128), BF16),
             pltpu.VMEM((n_y, tokens // 2, 128), BF16),
-            dma((2,)),
-            dma((2, far + 1, CHUNKS)),
-            dma((2, far + 1, CHUNKS)),
+            dma((10,)),
+            dma((4,)),
+            dma((2, far + 1, len(ORDER))),
+            dma((2, far + 1, len(ORDER))),
             dma((nz,)),
             dma((nz,)),
             dma((2, far + 1)),
@@ -504,10 +573,10 @@
             dma((2,)),
             dma((2,)),
             dma((2,)),
-            dma((NX,)),
-            dma((NX,)),
-            dma((n_y,)),
-            dma((n_y,)),
+            dma((n_y // 2, NX)),
+            dma((n_y // 2, NX)),
+            dma((n_y // 2, 2)),
+            dma((n_y // 2, 2)),
         ],
         compiler_params=pltpu.CompilerParams(
             collective_id=0, has_side_effects=True, vmem_limit_bytes=56 * 1024 * 1024

time: 99.4 us -> 86.8 us (0.87)
  the two profiles are of different devices: /device:TPU:16 before, /device:TPU:1 now
where the time goes in v3:
time: 86.8 us; the launch traced here: 85.1 us
  Pallas kernels  84.5 us (97%)
    pallas_call x1, Pallas kernels, on_device(): pl.pallas_call(functools.partial(kernel, n_tp, nz, units, cap), name='han...  81.7 us
    pallas_call x1, Pallas kernels, on_device(): pl.pallas_call(deliver, name='deliver', out_shape=[jax.ShapeDtypeStruct(v...  2.78 us

profile of v3, /device:TPU:1, one launch (start us, length us, event | category | flops | bytes accessed | tf_op | source)
XLA Modules:
  0.0 85.1 jit_solution(10737474952681287068)
XLA Ops:
  0.6 81.7 %hand_over.1 = (bf16[3,168,2048]{2,1,0:T(8,128)(2,1)S(1)}, bf16[3,168,2048]{2,1,0:T(8,128)(2,1)S(1)}, bf16[3,168,2048]{2,1,0:T(8,128)(2,1)S(1)}, bf16[64,504]{1,...) custom-call(f32[21,32,64]{2,1,0:T(8,128)} %bitcast.13, ...), custom_call_target="tpu_custom_call" | custom-call | tf_op jit(solution)/shard_map/hand_over/pallas_call | solution.py:538
  82.3 2.8 %deliver.1 = (bf16[3,168,2048]{2,1,0:T(8,128)(2,1)}, bf16[3,168,2048]{2,1,0:T(8,128)(2,1)}, bf16[3,168,2048]{2,1,0:T(8,128)(2,1)}, bf16[64,504]{1,0:T(8,128)(2,1...) custom-call(bf16[3,168,2048]{2,1,0:T(8,128)(2,1)S(1)} %get-tuple-element.21.refs_0_, ...), custom_call_target="tpu_custom_call" | custom-call | tf_op jit(solution)/shard_map/deliver/pallas_call | solution.py:585

commit v4 on v3

--- a/solution.py
+++ b/solution.py
@@ -88,13 +88,13 @@
         pl.semaphore_signal(barrier, inc=1, device_id={"tp": peer}, device_id_type=MESH)
         return 0
 
-    for other in (ahead, behind, twin):
-        pl.semaphore_signal(barrier, inc=1, device_id={"fs": other}, device_id_type=MESH)
-    lax.fori_loop(1, n_tp, greet, 0)
     vmem_in = (tg, tu, td, sg, su, sd, gain, tok, ids, scores)
     loads = [pltpu.make_async_copy(hbm_in[i], vmem_in[i], sem_in.at[i]) for i in range(10)]
     for load in loads:
         load.start()
+    for other in (ahead, behind, twin):
+        pl.semaphore_signal(barrier, inc=1, device_id={"fs": other}, device_id_type=MESH)
+    lax.fori_loop(1, n_tp, greet, 0)
     for i in (0, 1, 2, 3, 4, 5, 6):
         loads[i].wait()
 
@@ -157,14 +157,12 @@
     small_hop(1, 1, z).start()
     small_pair(z).start()
 
+    away = [(min(i, n_y - i) + min(j, NX - j), i, j) for i in range(n_y) for j in range(NX)]
     for h in (0, 1):
-
-        def send_weights(i, _, h=h):
-            peer = lax.rem(me + i, n_tp)
-            plane(send_a.at[h, peer], recv_a.at[h, me], sem_a, peer, 2 * h).start()
-            return 0
-
-        lax.fori_loop(1, n_tp, send_weights, 0)
+        for distance, i, j in sorted(away, reverse=True):
+            if distance:
+                peer = lax.rem(y + i, n_y) * NX + lax.rem(x + j, NX)
+                plane(send_a.at[h, peer], recv_a.at[h, me], sem_a, peer, 2 * h).start()
 
     def small_step(s):
         for d in (0, 1):
@@ -237,7 +235,7 @@
             device_id={"fs": twin}, device_id_type=MESH,
         )
 
-    early = far // 2
+    early = 2
     with jax.named_scope("small_early"):
         for i in range(1, early + 1):
             small_step(i)
@@ -334,15 +332,12 @@
                     def _(d=d, q=q, at=at):
                         hop(d, s + 1, q, at).start()
 
-            if n == 1:
-                with jax.named_scope("expert0"):
-                    expert(origin(0, s - 1))
-            if n == 2:
-
-                @pl.when(s > 1)
-                def _():
-                    with jax.named_scope("expert1"):
-                        expert(origin(1, s - 1))
+            if 0 < n < 3:
+
+                @pl.when(s == far - 1)
+                def _(d=n - 1):
+                    with jax.named_scope(f"expert_in{d}"):
+                        expert(origin(d, s - 1))
 
         for d in (0, 1):
             pair(origin(d, s)).start()
@@ -352,35 +347,38 @@
             with jax.named_scope("small"):
                 small_step(s + early)
 
-        @pl.when(s == far - early)
+        def one(i, _):
+            with jax.named_scope("expert"):
+                expert(lax.rem(z + nz + (s - 1) * (1 - 2 * i), nz))
+            return 0
+
+        @pl.when(s < far - 1)
         def _():
-            everything = small.at[:, 0]
-            done = pltpu.make_async_remote_copy(
-                src_ref=everything, dst_ref=everything,
-                send_sem=sem_spair.at[0], recv_sem=sem_spair.at[1],
-                device_id={"fs": twin}, device_id_type=MESH,
-            )
-            done.wait_send()
-            done.wait_recv()
-            with jax.named_scope("shared_rows"):
-                shared_rows()
-
-        @pl.when(s == far - early + 1)
-        def _():
-            with jax.named_scope("shared_acts"):
-                shared_acts()
+            lax.fori_loop(0, jnp.where(s == 1, 1, 2), one, 0)
 
         return 0
 
     lax.fori_loop(1, far, ring_step, 0)
+    with jax.named_scope("await_small"):
+        everything = small.at[:, 0]
+        done = pltpu.make_async_remote_copy(
+            src_ref=everything, dst_ref=everything,
+            send_sem=sem_spair.at[0], recv_sem=sem_spair.at[1],
+            device_id={"fs": twin}, device_id_type=MESH,
+        )
+        done.wait_send()
+        done.wait_recv()
+    with jax.named_scope("shared_rows"):
+        shared_rows()
+    opposite = lax.rem(z + far, nz)
     for d in (0, 1):
-        with jax.named_scope("expert_near_last"):
+        with jax.named_scope(f"expert_near{d}"):
             expert(origin(d, far - 1))
-    opposite = lax.rem(z + far, nz)
-    with jax.named_scope("arrive_last"):
-        for q in ORDER:
-            hop(0 if q in ORDER[:2] else 1, far, q, opposite).wait_recv()
-    pair(opposite).start()
+        if d == 0:
+            with jax.named_scope("arrive_last"):
+                for q in ORDER:
+                    hop(0 if q in ORDER[:2] else 1, far, q, opposite).wait_recv()
+            pair(opposite).start()
     with jax.named_scope("expert_last"):
         act = activated(opposite)
 
@@ -429,7 +427,10 @@
         with jax.named_scope("served"):
             lax.fori_loop(0, width // part, some, 0)
 
-    for g in range(groups - 1):
+    served(0)
+    with jax.named_scope("shared_acts"):
+        shared_acts()
+    for g in range(1, groups - 1):
         served(g)
 
     half = tokens // 2

time: 86.8 us -> 86.4 us (level); the launches traced: 85.1 us -> 86.3 us
  Pallas kernels: 84.5 us -> 85.6 us
    pallas_call x1, Pallas kernels: 81.7 us -> 82.8 us  [on_device(): pl.pallas_call(functools.partial(kernel, n_tp, nz, units, cap), name='han...]
where the time goes in v4:
time: 86.4 us; the launch traced here: 86.3 us
  Pallas kernels  85.6 us (99%)
    pallas_call x1, Pallas kernels, on_device(): pl.pallas_call(functools.partial(kernel, n_tp, nz, units, cap), name='han...  82.8 us
    pallas_call x1, Pallas kernels, on_device(): pl.pallas_call(deliver, name='deliver', out_shape=[jax.ShapeDtypeStruct(v...  2.78 us

profile of v4, /device:TPU:1, one launch (start us, length us, event | category | flops | bytes accessed | tf_op | source)
XLA Modules:
  0.0 86.3 jit_solution(13488844860951293211)
XLA Ops:
  0.6 82.8 %hand_over.1 = (bf16[3,168,2048]{2,1,0:T(8,128)(2,1)S(1)}, bf16[3,168,2048]{2,1,0:T(8,128)(2,1)S(1)}, bf16[3,168,2048]{2,1,0:T(8,128)(2,1)S(1)}, bf16[64,504]{1,...) custom-call(f32[21,32,64]{2,1,0:T(8,128)} %bitcast.13, ...), custom_call_target="tpu_custom_call" | custom-call | tf_op jit(solution)/shard_map/hand_over/pallas_call | solution.py:539
  83.5 2.8 %deliver.1 = (bf16[3,168,2048]{2,1,0:T(8,128)(2,1)}, bf16[3,168,2048]{2,1,0:T(8,128)(2,1)}, bf16[3,168,2048]{2,1,0:T(8,128)(2,1)}, bf16[64,504]{1,0:T(8,128)(2,1...) custom-call(bf16[3,168,2048]{2,1,0:T(8,128)(2,1)S(1)} %get-tuple-element.21.refs_0_, ...), custom_call_target="tpu_custom_call" | custom-call | tf_op jit(solution)/shard_map/deliver/pallas_call | solution.py:586

commit v5 on v3

--- a/solution.py
+++ b/solution.py
@@ -83,18 +83,20 @@
 
     barrier = pltpu.get_barrier_semaphore()
 
-    def greet(i, _):
-        peer = lax.rem(me + i, n_tp)
-        pl.semaphore_signal(barrier, inc=1, device_id={"tp": peer}, device_id_type=MESH)
-        return 0
-
-    for other in (ahead, behind, twin):
-        pl.semaphore_signal(barrier, inc=1, device_id={"fs": other}, device_id_type=MESH)
-    lax.fori_loop(1, n_tp, greet, 0)
+    away = [(min(i, n_y - i) + min(j, NX - j), i, j) for i in range(n_y) for j in range(NX)]
+    away = [
+        lax.rem(y + i, n_y) * NX + lax.rem(x + j, NX)
+        for distance, i, j in sorted(away, reverse=True)
+        if distance
+    ]
     vmem_in = (tg, tu, td, sg, su, sd, gain, tok, ids, scores)
     loads = [pltpu.make_async_copy(hbm_in[i], vmem_in[i], sem_in.at[i]) for i in range(10)]
     for load in loads:
         load.start()
+    for other in (ahead, behind, twin):
+        pl.semaphore_signal(barrier, inc=1, device_id={"fs": other}, device_id_type=MESH)
+    for peer in away:
+        pl.semaphore_signal(barrier, inc=1, device_id={"tp": peer}, device_id_type=MESH)
     for i in (0, 1, 2, 3, 4, 5, 6):
         loads[i].wait()
 
@@ -139,7 +141,7 @@
     def small_hop(d, s, at):
         return pltpu.make_async_remote_copy(
             src_ref=small.at[at, core], dst_ref=small.at[at, core],
-            send_sem=sem_small_s.at[d, s], recv_sem=sem_small_r.at[d, s],
+            send_sem=sem_small_s.at[d], recv_sem=sem_small_r.at[d, s - 1],
             device_id={"fs": ahead if d == 0 else behind}, device_id_type=MESH,
         )
 
@@ -158,13 +160,8 @@
     small_pair(z).start()
 
     for h in (0, 1):
-
-        def send_weights(i, _, h=h):
-            peer = lax.rem(me + i, n_tp)
+        for peer in away:
             plane(send_a.at[h, peer], recv_a.at[h, me], sem_a, peer, 2 * h).start()
-            return 0
-
-        lax.fori_loop(1, n_tp, send_weights, 0)
 
     def small_step(s):
         for d in (0, 1):
@@ -225,19 +222,20 @@
         piece = blocks.at[at, core, pl.ds(q * PIECE, PIECE)]
         return pltpu.make_async_remote_copy(
             src_ref=piece, dst_ref=piece,
-            send_sem=sem_ring_s.at[d, s, q], recv_sem=sem_ring_r.at[d, s, q],
+            send_sem=sem_ring_s.at[d, q], recv_sem=sem_ring_r.at[d, s - 1, q],
             device_id={"fs": ahead if d == 0 else behind}, device_id_type=MESH,
         )
 
-    def pair(at):
-        rel = lax.rem(at + nz - z, nz)
-        return pltpu.make_async_remote_copy(
-            src_ref=blocks.at[at, core], dst_ref=blocks.at[at, core],
-            send_sem=sem_pair_s.at[rel], recv_sem=sem_pair_r.at[rel],
+    def pair(at, q=None):
+        block = blocks.at[at, core]
+        piece = block if q is None else blocks.at[at, core, pl.ds(q * PIECE, PIECE)]
+        return pltpu.make_async_remote_copy(
+            src_ref=piece, dst_ref=piece,
+            send_sem=sem_pair_s, recv_sem=sem_pair_r.at[lax.rem(at + nz - z, nz)],
             device_id={"fs": twin}, device_id_type=MESH,
         )
 
-    early = far // 2
+    early = 3
     with jax.named_scope("small_early"):
         for i in range(1, early + 1):
             small_step(i)
@@ -253,22 +251,25 @@
         for q in ORDER[2 * h : 2 * h + 2]:
             for d in (0, 1):
                 hop(d, 1, q, z).start()
-    pair(z).start()
+            pair(z, q).start()
 
     def last_leg(d, q):
         return (q in ORDER[:2]) == (d == 0)
 
-    def activated(at):
+    def activated(*ats):
         with jax.named_scope("await_pair"):
-            pair(at).wait_recv()
-        pre = nt(rows[...], blocks[at].reshape(2 * ROW, width))
+            for at in ats:
+                pair(at).wait_recv()
+        w = jnp.concatenate([blocks[at].reshape(2 * ROW, width) for at in ats], axis=0)
+        pre = nt(rows[...], w)
         act = silu(pltpu.roll(pre, 2 * units, 1)) * pltpu.roll(pre, units, 1)
         unit = iota(act.shape, 1) & (ROW - 1)
         return jnp.where((unit >= 2 * units) & (unit < 3 * units), act, 0.0).astype(BF16)
 
-    def expert(at):
-        act = activated(at)
-        total[...] += nn(act, blocks[at].reshape(2 * ROW, width))
+    def expert(*ats):
+        act = activated(*ats)
+        w = jnp.concatenate([blocks[at].reshape(2 * ROW, width) for at in ats], axis=0)
+        total[...] += nn(act, w)
 
     def padded(v):
         spare = jnp.zeros((-hidden % 128, 128), F32)
@@ -334,55 +335,75 @@
                     def _(d=d, q=q, at=at):
                         hop(d, s + 1, q, at).start()
 
+                pair(at, q).start()
+
             if n == 1:
-                with jax.named_scope("expert0"):
-                    expert(origin(0, s - 1))
+
+                @pl.when(s + early <= far)
+                def _():
+                    with jax.named_scope("small"):
+                        small_step(s + early)
+
+                @pl.when(s == far - early + 1)
+                def _():
+                    with jax.named_scope("await_small"):
+                        everything = small.at[:, 0]
+                        done = pltpu.make_async_remote_copy(
+                            src_ref=everything, dst_ref=everything,
+                            send_sem=sem_spair.at[0], recv_sem=sem_spair.at[1],
+                            device_id={"fs": twin}, device_id_type=MESH,
+                        )
+                        done.wait_send()
+                        done.wait_recv()
+                    with jax.named_scope("shared_rows"):
+                        shared_rows()
+
             if n == 2:
 
-                @pl.when(s > 1)
+                @pl.when(s == far - 1)
                 def _():
-                    with jax.named_scope("expert1"):
-                        expert(origin(1, s - 1))
-
-        for d in (0, 1):
-            pair(origin(d, s)).start()
-
-        @pl.when(s + early <= far)
+                    with jax.named_scope("expert_in"):
+                        expert(origin(0, s - 1), origin(1, s - 1))
+
+        @pl.when(s == 1)
         def _():
-            with jax.named_scope("small"):
-                small_step(s + early)
-
-        @pl.when(s == far - early)
+            with jax.named_scope("expert_own"):
+                expert(z)
+
+        @pl.when((s > 1) & (s < far - 1))
         def _():
-            everything = small.at[:, 0]
-            done = pltpu.make_async_remote_copy(
-                src_ref=everything, dst_ref=everything,
-                send_sem=sem_spair.at[0], recv_sem=sem_spair.at[1],
-                device_id={"fs": twin}, device_id_type=MESH,
-            )
-            done.wait_send()
-            done.wait_recv()
-            with jax.named_scope("shared_rows"):
-                shared_rows()
-
-        @pl.when(s == far - early + 1)
-        def _():
-            with jax.named_scope("shared_acts"):
-                shared_acts()
+            with jax.named_scope("expert"):
+                expert(origin(0, s - 1), origin(1, s - 1))
 
         return 0
 
     lax.fori_loop(1, far, ring_step, 0)
-    for d in (0, 1):
-        with jax.named_scope("expert_near_last"):
-            expert(origin(d, far - 1))
     opposite = lax.rem(z + far, nz)
+    with jax.named_scope("shared_acts"):
+        shared_acts()
+    with jax.named_scope("expert_near"):
+        expert(origin(0, far - 1), origin(1, far - 1))
     with jax.named_scope("arrive_last"):
         for q in ORDER:
             hop(0 if q in ORDER[:2] else 1, far, q, opposite).wait_recv()
-    pair(opposite).start()
+            pair(opposite, q).start()
     with jax.named_scope("expert_last"):
         act = activated(opposite)
+
+    def sent(ref, sem):
+        pltpu.make_async_remote_copy(
+            src_ref=ref, dst_ref=ref, send_sem=sem, recv_sem=sem_pair_r.at[0],
+            device_id={"fs": twin}, device_id_type=MESH,
+        ).wait_send()
+
+    def drain():
+        for d in (0, 1):
+            for q in ORDER:
+                hops = far - 1 + last_leg(d, q)
+                sent(blocks.at[pl.ds(0, hops), 0, pl.ds(0, PIECE)], sem_ring_s.at[d, q])
+            sent(small.at[pl.ds(0, far - d), 0], sem_small_s.at[d])
+        sent(blocks.at[:, 0], sem_pair_s)
+        sent(send_x.at[pl.ds(0, NX - 1)], sem_x_s)
 
     w = slot_weight[...]
     pairs = n_y // 2
@@ -396,7 +417,7 @@
         to = lax.rem(x + i, NX)
         return pltpu.make_async_remote_copy(
             src_ref=send_x.at[to, k], dst_ref=recv_x.at[x, k],
-            send_sem=sem_x_s.at[k, i], recv_sem=sem_x_r.at[k, i],
+            send_sem=sem_x_s, recv_sem=sem_x_r.at[k, i],
             device_id={"tp": y * NX + to}, device_id_type=MESH,
         )
 
@@ -440,14 +461,14 @@
         to = 2 * quarter(k) + (1 - odd if last else h)
         return pltpu.make_async_remote_copy(
             src_ref=send_y.at[to], dst_ref=recv_y.at[y],
-            send_sem=sem_y_s.at[k, h], recv_sem=sem_y_r.at[k, 0 if last else odd],
+            send_sem=sem_y_s, recv_sem=sem_y_r.at[k, 0 if last else odd],
             device_id={"tp": to * NX + x}, device_id_type=MESH,
         )
 
     def col_arrival(k, h):
         return pltpu.make_async_remote_copy(
             src_ref=recv_y.at[0], dst_ref=recv_y.at[0],
-            send_sem=sem_y_s.at[k, h], recv_sem=sem_y_r.at[k, h],
+            send_sem=sem_y_s, recv_sem=sem_y_r.at[k, h],
             device_id={"tp": lax.rem(me + 1, n_tp)}, device_id_type=MESH,
         )
 
@@ -466,6 +487,8 @@
                 col_copy(k, h).start()
     recv_y[y] = send_y[y]
     served(groups - 1)
+    with jax.named_scope("drain"):
+        drain()
 
     with jax.named_scope("await_act"):
         plane_done(acts, sem_act)
@@ -479,31 +502,7 @@
     mixed = mixed.T
     o_mix[...] = jnp.concatenate([mixed[:64], mixed[64:]], axis=1).astype(BF16)
 
-    for d in (0, 1):
-        for q in ORDER:
-
-            def sent(s, _, d=d, q=q):
-                hop(d, s, q, z).wait_send()
-                return 0
-
-            lax.fori_loop(1, far + (1 if last_leg(d, q) else 0), sent, 0)
-
-        def small_sent(s, _, d=d):
-            small_hop(d, s, z).wait_send()
-            return 0
-
-        lax.fori_loop(1, far + (1 if d == 0 else 0), small_sent, 0)
-
-    def pair_sent(i, _):
-        pair(i).wait_send()
-        return 0
-
-    lax.fori_loop(0, nz, pair_sent, 0)
-    for k in range(pairs):
-        for i in range(1, NX):
-            row_copy(k, i).wait_send()
-    for k, h in y_copies:
-        col_copy(k, h).wait_send()
+    sent(send_y.at[pl.ds(0, n_y - 1)], sem_y_s)
 
 
 def deliver(*refs):
@@ -564,18 +563,18 @@
             pltpu.VMEM((n_y, tokens // 2, 128), BF16),
             dma((10,)),
             dma((4,)),
-            dma((2, far + 1, len(ORDER))),
-            dma((2, far + 1, len(ORDER))),
+            dma((2, len(ORDER))),
+            dma((2, far, len(ORDER))),
+            dma(()),
             dma((nz,)),
-            dma((nz,)),
-            dma((2, far + 1)),
-            dma((2, far + 1)),
+            dma((2,)),
+            dma((2, far)),
             dma((2,)),
             dma((2,)),
             dma((2,)),
+            dma(()),
             dma((n_y // 2, NX)),
-            dma((n_y // 2, NX)),
-            dma((n_y // 2, 2)),
+            dma(()),
             dma((n_y // 2, 2)),
         ],
         compiler_params=pltpu.CompilerParams(

time: 86.8 us -> 83.5 us (0.962)
  Pallas kernels: 84.5 us -> 82 us
    pallas_call x1, Pallas kernels: 81.7 us -> 79.2 us  [on_device(): pl.pallas_call(functools.partial(kernel, n_tp, nz, units, cap), name='han...]
where the time goes in v5:
time: 83.5 us; the launch traced here: 82.6 us
  Pallas kernels  82 us (98%)
    pallas_call x1, Pallas kernels, on_device(): pl.pallas_call(functools.partial(kernel, n_tp, nz, units, cap), name='han...  79.2 us
    pallas_call x1, Pallas kernels, on_device(): pl.pallas_call(deliver, name='deliver', out_shape=[jax.ShapeDtypeStruct(v...  2.78 us

profile of v5, /device:TPU:1, one launch (start us, length us, event | category | flops | bytes accessed | tf_op | source)
XLA Modules:
  0.0 82.6 jit_solution(7329329583943089855)
XLA Ops:
  0.6 79.2 %hand_over.1 = (bf16[3,168,2048]{2,1,0:T(8,128)(2,1)S(1)}, bf16[3,168,2048]{2,1,0:T(8,128)(2,1)S(1)}, bf16[3,168,2048]{2,1,0:T(8,128)(2,1)S(1)}, bf16[64,504]{1,...) custom-call(f32[21,32,64]{2,1,0:T(8,128)} %bitcast.13, ...), custom_call_target="tpu_custom_call" | custom-call | tf_op jit(solution)/shard_map/hand_over/pallas_call | solution.py:537
  79.9 2.8 %deliver.1 = (bf16[3,168,2048]{2,1,0:T(8,128)(2,1)}, bf16[3,168,2048]{2,1,0:T(8,128)(2,1)}, bf16[3,168,2048]{2,1,0:T(8,128)(2,1)}, bf16[64,504]{1,0:T(8,128)(2,1...) custom-call(bf16[3,168,2048]{2,1,0:T(8,128)(2,1)S(1)} %get-tuple-element.21.refs_0_, ...), custom_call_target="tpu_custom_call" | custom-call | tf_op jit(solution)/shard_map/deliver/pallas_call | solution.py:584

commit v6 on v5

--- a/solution.py
+++ b/solution.py
@@ -237,9 +237,12 @@
 
     early = 3
     with jax.named_scope("small_early"):
-        for i in range(1, early + 1):
+        for i in range(1, early):
             small_step(i)
     for h in (0, 1):
+        if h:
+            with jax.named_scope("small_between"):
+                small_step(early)
         with jax.named_scope(f"await_weights{h}"):
             plane_done(recv_a.at[h], sem_a, 2 * h)
         with jax.named_scope("unpack"):
@@ -344,7 +347,9 @@
                     with jax.named_scope("small"):
                         small_step(s + early)
 
-                @pl.when(s == far - early + 1)
+            if n == 3:
+
+                @pl.when(s == far - early)
                 def _():
                     with jax.named_scope("await_small"):
                         everything = small.at[:, 0]
@@ -381,12 +386,16 @@
     opposite = lax.rem(z + far, nz)
     with jax.named_scope("shared_acts"):
         shared_acts()
-    with jax.named_scope("expert_near"):
-        expert(origin(0, far - 1), origin(1, far - 1))
-    with jax.named_scope("arrive_last"):
+
+    def take_last():
         for q in ORDER:
             hop(0 if q in ORDER[:2] else 1, far, q, opposite).wait_recv()
             pair(opposite, q).start()
+
+    pl.when(core == 1)(take_last)
+    with jax.named_scope("expert_near"):
+        expert(origin(0, far - 1), origin(1, far - 1))
+    pl.when(core == 0)(take_last)
     with jax.named_scope("expert_last"):
         act = activated(opposite)
 
@@ -507,7 +516,12 @@
 
 def deliver(*refs):
     n = (len(refs) - 1) // 2
-    copies = [pltpu.make_async_copy(refs[i], refs[n + i], refs[-1].at[i]) for i in range(n)]
+    copies = []
+    for i in range(n):
+        parts = range(refs[i].shape[0]) if i < 3 else (None,)
+        for g in parts:
+            ends = [ref if g is None else ref.at[g] for ref in (refs[i], refs[n + i])]
+            copies.append(pltpu.make_async_copy(*ends, refs[-1].at[len(copies)]))
     for copy in copies:
         copy.start()
     for copy in copies:
@@ -587,7 +601,7 @@
         out_shape=[jax.ShapeDtypeStruct(v.shape, v.dtype) for v in outs],
         in_specs=[vm] * 7,
         out_specs=[hbm] * 7,
-        scratch_shapes=[dma((7,))],
+        scratch_shapes=[dma((3 * groups + 4,))],
         compiler_params=pltpu.CompilerParams(vmem_limit_bytes=1024 * 1024),
     )(*[pltpu.with_memory_space_constraint(v, pltpu.VMEM) for v in outs])
     full = [v.reshape(1, hidden, width) for v in outs[:3]]

time: 83.5 us -> 81.8 us (0.980)
  Pallas kernels: 82 us -> 81 us
    pallas_call x1, Pallas kernels: 79.2 us -> 78.2 us  [on_device(): pl.pallas_call(functools.partial(kernel, n_tp, nz, units, cap), name='han...]
where the time goes in v6:
time: 81.8 us; the launch traced here: 81.6 us
  Pallas kernels  81 us (99%)
    pallas_call x1, Pallas kernels, on_device(): pl.pallas_call(functools.partial(kernel, n_tp, nz, units, cap), name='han...  78.2 us
    pallas_call x1, Pallas kernels, on_device(): pl.pallas_call(deliver, name='deliver', out_shape=[jax.ShapeDtypeStruct(v...  2.79 us

profile of v6, /device:TPU:1, one launch (start us, length us, event | category | flops | bytes accessed | tf_op | source)
XLA Modules:
  0.0 81.6 jit_solution(17485909860082648243)
XLA Ops:
  0.6 78.2 %hand_over.1 = (bf16[3,168,2048]{2,1,0:T(8,128)(2,1)S(1)}, bf16[3,168,2048]{2,1,0:T(8,128)(2,1)S(1)}, bf16[3,168,2048]{2,1,0:T(8,128)(2,1)S(1)}, bf16[64,504]{1,...) custom-call(f32[21,32,64]{2,1,0:T(8,128)} %bitcast.13, ...), custom_call_target="tpu_custom_call" | custom-call | tf_op jit(solution)/shard_map/hand_over/pallas_call | solution.py:551
  78.8 2.8 %deliver.1 = (bf16[3,168,2048]{2,1,0:T(8,128)(2,1)}, bf16[3,168,2048]{2,1,0:T(8,128)(2,1)}, bf16[3,168,2048]{2,1,0:T(8,128)(2,1)}, bf16[64,504]{1,0:T(8,128)(2,1...) custom-call(bf16[3,168,2048]{2,1,0:T(8,128)(2,1)S(1)} %get-tuple-element.21.refs_0_, ...), custom_call_target="tpu_custom_call" | custom-call | tf_op jit(solution)/shard_map/deliver/pallas_call | solution.py:598

commit v7 on v6

--- a/solution.py
+++ b/solution.py
@@ -388,7 +388,7 @@
         shared_acts()
 
     def take_last():
-        for q in ORDER:
+        for q in (*ORDER[::2], *ORDER[1::2]):
             hop(0 if q in ORDER[:2] else 1, far, q, opposite).wait_recv()
             pair(opposite, q).start()
 
@@ -483,12 +483,11 @@
 
     y_copies = [(k, h) for k in range(pairs) for h in (0, 1) if k < pairs - 1 or h == 0]
     for k in range(pairs):
-        with jax.named_scope(f"await_x{k}"):
-            for i in range(1, NX):
-                row_copy(k, i).wait_recv()
-        acc = jnp.zeros((tokens, 128), F32)
-        for i in range(NX):
-            acc += nn(spread[i], recv_x[i, k])
+        acc = nn(spread[x], recv_x[x, k])
+        for i in range(1, NX):
+            row_copy(k, i).wait_recv()
+            source = lax.rem(x + NX - i, NX)
+            acc += nn(spread[source], recv_x[source, k])
         for h, v in enumerate(halves(acc[:half], acc[half:])):
             send_y[2 * quarter(k) + h] = v.astype(BF16)
         for h in (0, 1):

time: 81.8 us -> 81.9 us (level)
  no operation moved by 1% of the time
where the time goes in v7:
time: 81.9 us; the launch traced here: 81.7 us
  Pallas kernels  81 us (99%)
    pallas_call x1, Pallas kernels, on_device(): pl.pallas_call(functools.partial(kernel, n_tp, nz, units, cap), name='han...  78.2 us
    pallas_call x1, Pallas kernels, on_device(): pl.pallas_call(deliver, name='deliver', out_shape=[jax.ShapeDtypeStruct(v...  2.79 us

profile of v7, /device:TPU:1, one launch (start us, length us, event | category | flops | bytes accessed | tf_op | source)
XLA Modules:
  0.0 81.7 jit_solution(17565918366415830136)
XLA Ops:
  0.6 78.2 %hand_over.1 = (bf16[3,168,2048]{2,1,0:T(8,128)(2,1)S(1)}, bf16[3,168,2048]{2,1,0:T(8,128)(2,1)S(1)}, bf16[3,168,2048]{2,1,0:T(8,128)(2,1)S(1)}, bf16[64,504]{1,...) custom-call(f32[21,32,64]{2,1,0:T(8,128)} %bitcast.13, ...), custom_call_target="tpu_custom_call" | custom-call | tf_op jit(solution)/shard_map/hand_over/pallas_call | solution.py:550
  78.9 2.8 %deliver.1 = (bf16[3,168,2048]{2,1,0:T(8,128)(2,1)}, bf16[3,168,2048]{2,1,0:T(8,128)(2,1)}, bf16[3,168,2048]{2,1,0:T(8,128)(2,1)}, bf16[64,504]{1,0:T(8,128)(2,1...) custom-call(bf16[3,168,2048]{2,1,0:T(8,128)(2,1)S(1)} %get-tuple-element.21.refs_0_, ...), custom_call_target="tpu_custom_call" | custom-call | tf_op jit(solution)/shard_map/deliver/pallas_call | solution.py:597
